TPU v7x, 32 devices: a whole 2x2x4 slice. The times are simulated.
32 devices in a mesh: ep: 8 (over z, core), tp: 4 (over y, x).
Axes of the slice: x: 2, y: 2, z: 4, core: 2. Of those that a mesh axis runs over, the one named last changes fastest.
Arguments:
- tokens: bfloat16 [128, 2048], P('ep'), may hold values from -6 to 6
- old_state: float32 [128, 16, 128, 128], P('ep', 'tp'), may hold values from -2 to 2
- lower_bound: float32 [2048], P('tp'), may hold values from 0.05 to 0.95
- head_gain: float32 [2048], P('tp'), may hold values from 0.1 to 1.9
- norm_gains: float32 [4, 2048], replicated, may hold values from 0.1 to 1.9
- w_query: bfloat16 [2048, 2048], P('ep', 'tp'), may hold values from -0.125 to 0.125
- w_forget: bfloat16 [2048, 2048], P('ep', 'tp'), may hold values from -0.125 to 0.125
- w_value: bfloat16 [2048, 2048], P('ep', 'tp'), may hold values from -0.125 to 0.125
- w_outgate: bfloat16 [2048, 2048], P('ep', 'tp'), may hold values from -0.125 to 0.125
- w_mix_out: bfloat16 [2048, 2048], P('tp', 'ep'), may hold values from -0.125 to 0.125
- routes: int32 [128, 2], P('ep'), may hold values from 0 to 7, all different within a row; in each aligned block of 16 rows (0 to 15, 16 to 31, ...) at most 8 rows name the same one
- route_scores: float32 [128, 2], P('ep'), may hold values from -6 to 6
- w_exp_gate: bfloat16 [8, 2048, 3584], P('ep', None, 'tp'), may hold values from -0.125 to 0.125
- w_exp_up: bfloat16 [8, 2048, 3584], P('ep', None, 'tp'), may hold values from -0.125 to 0.125
- w_exp_down: bfloat16 [8, 3584, 2048], P('ep', 'tp'), may hold values from -0.75 to 0.75
- w_dense_gate: bfloat16 [2048, 6144], P('ep', 'tp'), may hold values from -0.125 to 0.125
- w_dense_up: bfloat16 [2048, 6144], P('ep', 'tp'), may hold values from -0.125 to 0.125
- w_dense_down: bfloat16 [6144, 2048], P('tp', 'ep'), may hold values from -0.75 to 0.75
- dense_mix: bfloat16 [2048], replicated, may hold values from -0.125 to 0.125
Outputs:
- layer_out: bfloat16 [128, 2048], P('ep', 'tp')
- new_state: float32 [128, 16, 128, 128], P('ep', 'tp')
Inputs may be any that keep to these rules, and one draw needn't show every extreme that they name: `routes`: each row names 2 different experts. In each aligned block of 16 rows no expert is named by more than 8 rows, and in every draw some expert is named by exactly 8 rows of some block.
All inputs are finite; a program needn't handle non-finite values.
Results may differ from a plain program's by a relative error of at most 0.025.
Values may be sent and summed in bfloat16 or wider, within the bound.
A program may use at most 64 MiB of HBM per device.

v0:
```python
import jax
import jax.numpy as jnp
from jax import lax
from jax.experimental import pallas as pl
from jax.experimental.pallas import tpu as pltpu
from jax.sharding import PartitionSpec as P

EPS = 1e-06


def rms_scale(values):
    return lax.rsqrt(jnp.mean(values * values, axis=-1, keepdims=True) + EPS)


def body(
    tokens,
    old_state,
    lower_bound,
    head_gain,
    norm_gains,
    w_query,
    w_forget,
    w_value,
    w_outgate,
    w_mix_out,
    routes,
    route_scores,
    w_exp_gate,
    w_exp_up,
    w_exp_down,
    w_dense_gate,
    w_dense_up,
    w_dense_down,
    dense_mix,
):
    highest = lax.Precision.HIGHEST
    seqs, width = tokens.shape
    column_index = lax.axis_index("tp")
    part_width = width // lax.axis_size("tp")
    resid = tokens.astype(jnp.float32)
    normed = (resid * rms_scale(resid) * norm_gains[0]).astype(jnp.bfloat16)
    in_weights = jnp.concatenate([w_query, w_forget, w_value, w_outgate], axis=1)
    mix_rows = lax.all_to_all(normed, "ep", split_axis=1, concat_axis=0, tiled=True)
    projected = lax.psum_scatter(
        jnp.dot(mix_rows, in_weights, preferred_element_type=jnp.float32).astype(jnp.bfloat16),
        "ep",
        scatter_dimension=0,
        tiled=True,
    ).astype(jnp.float32)
    query_raw, forget_raw, value, out_gate = jnp.split(projected, 4, axis=1)
    heads = old_state.shape[1]
    head_size = old_state.shape[2]
    shape_heads = (seqs, heads, head_size)
    forget = lower_bound + (1.0 - lower_bound) * jax.nn.sigmoid(forget_raw)
    key_in = (1.0 - lower_bound) * jax.nn.sigmoid(-forget_raw)
    new_state = forget.reshape(shape_heads)[..., None] * old_state + key_in.reshape(shape_heads)[
        ..., None
    ] * value.reshape(seqs, heads, 1, head_size)
    query = jax.nn.silu(query_raw).reshape(shape_heads)
    read = jnp.einsum("thk,thkv->thv", query, new_state, precision=highest)
    gated = (
        read
        * rms_scale(read)
        * head_gain.reshape(heads, head_size)
        * jax.nn.silu(out_gate).reshape(shape_heads)
    )
    mixed_heads = gated.reshape(seqs, heads * head_size).astype(jnp.bfloat16)
    mix_part = jnp.dot(
        mixed_heads,
        lax.all_gather(w_mix_out, "ep", axis=1, tiled=True),
        preferred_element_type=jnp.float32,
    ).astype(jnp.bfloat16)
    mix_part = lax.optimization_barrier(mix_part).astype(jnp.float32)
    mix_out = lax.psum(mix_part.astype(jnp.bfloat16), "tp")
    mix_wide = lax.optimization_barrier(mix_out).astype(jnp.float32)
    after_mix = resid + mix_wide * rms_scale(mix_wide) * norm_gains[1]
    ffn_in = (after_mix * rms_scale(after_mix) * norm_gains[2]).astype(jnp.bfloat16)
    experts = lax.axis_size("ep")
    topk = routes.shape[1]
    capacity = max(2, 2 * seqs * topk // experts)
    flat_routes = routes.reshape(-1)
    onehot = (flat_routes[:, None] == jnp.arange(experts, dtype=jnp.int32)[None, :]).astype(
        jnp.int32
    )
    before = jnp.cumsum(onehot, axis=0) - onehot
    slots = jnp.sum(onehot * before, axis=1)
    cells = flat_routes * capacity + slots
    placed = cells[None, :] == jnp.arange(experts * capacity, dtype=jnp.int32)[:, None]
    repeated = jnp.repeat(ffn_in, topk, axis=0)
    outgoing = jnp.dot(placed.astype(jnp.bfloat16), repeated, preferred_element_type=jnp.float32)
    outgoing = outgoing.astype(jnp.bfloat16).reshape(experts, capacity, width)
    arrived = lax.all_to_all(outgoing, "ep", split_axis=0, concat_axis=0, tiled=True)
    sources, items, _ = arrived.shape
    expert_rows = arrived.reshape(sources * items, width)
    gate_pre = jnp.dot(expert_rows, w_exp_gate[0], preferred_element_type=jnp.float32)
    up_pre = jnp.dot(expert_rows, w_exp_up[0], preferred_element_type=jnp.float32)
    hidden = (jax.nn.silu(gate_pre) * up_pre).astype(jnp.bfloat16)
    partial_rows = jnp.dot(hidden, w_exp_down[0], preferred_element_type=jnp.float32).astype(
        jnp.bfloat16
    )
    partial_rows = lax.optimization_barrier(partial_rows).astype(jnp.float32)
    partial_rows = partial_rows.reshape(sources, items, width)
    summed = lax.psum_scatter(
        partial_rows.astype(jnp.bfloat16), "tp", scatter_dimension=2, tiled=True
    )
    returned = lax.all_to_all(summed, "ep", split_axis=0, concat_axis=0, tiled=True)
    first = jax.nn.sigmoid(route_scores[:, 0] - route_scores[:, 1])
    second = jax.nn.sigmoid(route_scores[:, 1] - route_scores[:, 0])
    route_weight = jnp.stack([first, second], axis=1).reshape(-1)
    weight_table = jnp.sum(
        (placed.astype(jnp.float32) * route_weight[None, :]).reshape(
            experts * capacity, seqs, topk
        ),
        axis=2,
    )
    expert_sum = jnp.dot(
        weight_table.T,
        returned.reshape(experts * capacity, part_width).astype(jnp.float32),
        precision=highest,
    )
    dense_weights = jnp.concatenate([w_dense_gate, w_dense_up], axis=1)
    dense_rows = lax.all_to_all(ffn_in, "ep", split_axis=1, concat_axis=0, tiled=True)
    dense_pre = lax.psum_scatter(
        jnp.dot(dense_rows, dense_weights, preferred_element_type=jnp.float32).astype(jnp.bfloat16),
        "ep",
        scatter_dimension=0,
        tiled=True,
    ).astype(jnp.float32)
    dense_gate_pre, dense_up_pre = jnp.split(dense_pre, 2, axis=1)
    dense_hidden = (jax.nn.silu(dense_gate_pre) * dense_up_pre).astype(jnp.bfloat16)
    dense_partial = jnp.dot(
        dense_hidden,
        lax.all_gather(w_dense_down, "ep", axis=1, tiled=True),
        preferred_element_type=jnp.float32,
    )
    dense_out = lax.psum_scatter(
        dense_partial.astype(jnp.bfloat16), "tp", scatter_dimension=1, tiled=True
    ).astype(jnp.float32)
    mix_weight = jax.nn.sigmoid(jnp.dot(ffn_in, dense_mix, preferred_element_type=jnp.float32))
    ffn_out = expert_sum + mix_weight[:, None] * dense_out
    squares = lax.psum(jnp.sum(ffn_out * ffn_out, axis=1), "tp")
    out_scale = lax.rsqrt(squares / width + EPS)
    gain_part = lax.dynamic_slice_in_dim(norm_gains[3], column_index * part_width, part_width, 0)
    resid_part = lax.dynamic_slice_in_dim(after_mix, column_index * part_width, part_width, 1)
    layer_out = (resid_part + ffn_out * out_scale[:, None] * gain_part).astype(jnp.bfloat16)
    return (layer_out, new_state)


def dot32(a, b):
    return jnp.dot(a, b, preferred_element_type=jnp.float32)


MESH = pl.DeviceIdType.MESH


def offsets_of(group, n_ep, n_tp):
    if group == "ep":
        return [(de, 0) for de in range(n_ep)]
    if group == "tp":
        return [(0, dt) for dt in range(n_tp)]
    return [(de, dt) for de in range(n_ep) for dt in range(n_tp)]


def enter(group, n_ep, n_tp):
    me_e, me_t = lax.axis_index("ep"), lax.axis_index("tp")
    barrier = pltpu.get_barrier_semaphore()
    offsets = offsets_of(group, n_ep, n_tp)[1:]
    for de, dt in offsets:
        pl.semaphore_signal(
            barrier,
            inc=1,
            device_id=(lax.rem(me_e + de, n_ep), lax.rem(me_t + dt, n_tp)),
            device_id_type=MESH,
        )
    pl.semaphore_wait(barrier, len(offsets))


def begin(p, x, o, mode, n_ep, n_tp, send, recv):
    me_e, me_t = lax.axis_index("ep"), lax.axis_index("tp")
    ratio = n_ep // n_tp
    waits = []
    if mode == "cols":
        t = me_e // ratio
        slot = lax.rem(me_e, ratio) * n_tp + me_t
        dst = o.at[lax.rem(me_e, ratio), me_t]
        for de in range(n_ep):
            e = lax.rem(me_e + de, n_ep)
            remote = pltpu.make_async_remote_copy(
                src_ref=x.at[e],
                dst_ref=dst,
                send_sem=send.at[p, de],
                recv_sem=recv.at[p, slot],
                device_id=(e, t),
                device_id_type=MESH,
            )
            if de == 0:
                own = pltpu.make_async_copy(x.at[e], dst, recv.at[p, slot])
                pl.when(t == me_t)(own.start)
                pl.when(t != me_t)(remote.start)
                waits.append(lambda remote=remote: pl.when(t != me_t)(remote.wait_send))
            else:
                remote.start()
                waits.append(remote.wait_send)
            arrival = pltpu.make_async_copy(
                x.at[0], o.at[de // n_tp, de % n_tp], recv.at[p, de]
            )
            waits.append(arrival.wait)
    else:
        group = {"a2a": "ep", "bcast": "ep", "bcast_tp": "tp", "all": "all"}[mode]
        for index, (de, dt) in enumerate(offsets_of(group, n_ep, n_tp)):
            e, t = lax.rem(me_e + de, n_ep), lax.rem(me_t + dt, n_tp)
            if mode == "a2a":
                src, dst = x.at[e], o.at[me_e]
            elif mode == "bcast":
                src, dst = x, o.at[me_e]
            elif mode == "bcast_tp":
                src, dst = x, o.at[me_t]
            else:
                src = x.at[e, t] if len(x.shape) == 4 else x.at[e]
                dst = o.at[me_e, me_t]
            if index == 0:
                copy = pltpu.make_async_copy(src, dst, recv.at[p, 0])
            else:
                copy = pltpu.make_async_remote_copy(
                    src_ref=src,
                    dst_ref=dst,
                    send_sem=send.at[p, index],
                    recv_sem=recv.at[p, index],
                    device_id=(e, t),
                    device_id_type=MESH,
                )
            copy.start()
            waits.append(copy.wait)

    def finish():
        for wait in waits:
            wait()

    return finish


def pair_reduce(p, p2, x, y, z, o, n_ep, n_tp, send, recv):
    me_e, me_t = lax.axis_index("ep"), lax.axis_index("tp")
    half = n_ep // 2
    q, c = me_e // 2, lax.rem(me_e, 2)
    partner = 2 * q + 1 - c
    turns = [lax.rem(q + 1 + k, half) for k in range(half)]
    firsts = []
    for k, kk in enumerate(turns):
        copy = pltpu.make_async_remote_copy(
            src_ref=x.at[2 * kk + 1 - c],
            dst_ref=y.at[kk],
            send_sem=send.at[p, k],
            recv_sem=recv.at[p, k],
            device_id=(partner, me_t),
            device_id_type=MESH,
        )
        copy.start()
        firsts.append(copy)
    seconds = []
    for k, kk in enumerate(turns):
        firsts[k].wait()
        z[kk] = (x[2 * kk + c].astype(jnp.float32) + y[kk].astype(jnp.float32)).astype(z.dtype)
        if k == half - 1:
            copy = pltpu.make_async_copy(z.at[kk], o.at[q], recv.at[p2, k])
        else:
            copy = pltpu.make_async_remote_copy(
                src_ref=z.at[kk],
                dst_ref=o.at[q],
                send_sem=send.at[p2, k],
                recv_sem=recv.at[p2, k],
                device_id=(2 * kk + c, me_t),
                device_id_type=MESH,
            )
        copy.start()
        seconds.append(copy)

    def finish():
        for copy in seconds:
            copy.wait()

    return finish


def pair_gather(p, p2, x, o, n_ep, n_tp, send, recv):
    me_e, me_t = lax.axis_index("ep"), lax.axis_index("tp")
    half = n_ep // 2
    q, c = me_e // 2, lax.rem(me_e, 2)
    partner = 2 * q + 1 - c
    crossing = []
    for k in range(half):
        e = partner if k == 0 else 2 * lax.rem(q + k, half) + c
        copy = pltpu.make_async_remote_copy(
            src_ref=x,
            dst_ref=o.at[me_e],
            send_sem=send.at[p, k],
            recv_sem=recv.at[p, k],
            device_id=(e, me_t),
            device_id_type=MESH,
        )
        copy.start()
        crossing.append(copy)
    own = pltpu.make_async_copy(x, o.at[me_e], recv.at[p, half])
    own.start()
    handed = []
    for k in range(1, half):
        crossing[k].wait_recv()
        block = o.at[2 * lax.rem(q + half - k, half) + c]
        copy = pltpu.make_async_remote_copy(
            src_ref=block,
            dst_ref=block,
            send_sem=send.at[p2, k],
            recv_sem=recv.at[p2, k],
            device_id=(partner, me_t),
            device_id_type=MESH,
        )
        copy.start()
        handed.append(copy)
    own.wait()
    crossing[0].wait()
    for copy in crossing[1:]:
        copy.wait_send()
    for copy in handed:
        copy.wait()


def silu(x):
    return x * jax.nn.sigmoid(x)


def project(tokens, norm_gains, weights, n_ep, n_tp):
    seqs, width = tokens.shape
    block = width // n_ep
    cols = weights[0].shape[1]
    bf16, f32 = jnp.bfloat16, jnp.float32

    def kernel(tok, gains, w0, w1, w2, w3, out, x1, r1, x2, y2, z2, r2, send, recv):
        resid = tok[...].astype(f32)
        normed = (resid * rms_scale(resid) * gains[0:1, :]).astype(bf16)
        for e in range(n_ep):
            x1[e] = normed[:, e * block : (e + 1) * block]
        enter("ep", n_ep, n_tp)
        begin(0, x1, r1, "a2a", n_ep, n_tp, send, recv)()
        rows = r1[...].reshape(n_ep * seqs, block)
        for i, w in enumerate((w0, w1, w2, w3)):
            part = dot32(rows, w[...]).astype(bf16)
            for e in range(n_ep):
                x2[e, :, i * cols : (i + 1) * cols] = part[e * seqs : (e + 1) * seqs]
        pair_reduce(1, 2, x2, y2, z2, r2, n_ep, n_tp, send, recv)()
        for i in range(4):
            total = jnp.zeros((seqs, cols), f32)
            for e in range(n_ep // 2):
                total += r2[e, :, i * cols : (i + 1) * cols].astype(f32)
            out[:, i * cols : (i + 1) * cols] = total

    vmem = pl.BlockSpec(memory_space=pltpu.VMEM)
    return pl.pallas_call(
        kernel,
        out_shape=jax.ShapeDtypeStruct((seqs, 4 * cols), f32),
        in_specs=[vmem] * 6,
        out_specs=vmem,
        scratch_shapes=[
            pltpu.VMEM((n_ep, seqs, block), bf16),
            pltpu.VMEM((n_ep, seqs, block), bf16),
            pltpu.VMEM((n_ep, seqs, 4 * cols), bf16),
            pltpu.VMEM((n_ep // 2, seqs, 4 * cols), bf16),
            pltpu.VMEM((n_ep // 2, seqs, 4 * cols), bf16),
            pltpu.VMEM((n_ep // 2, seqs, 4 * cols), bf16),
            pltpu.SemaphoreType.DMA((3, n_ep)),
            pltpu.SemaphoreType.DMA((3, n_ep)),
        ],
        compiler_params=pltpu.CompilerParams(collective_id=1, has_side_effects=True),
        name="project",
    )(tokens, norm_gains, *weights)


def finish_layer(
    mixed, tokens, norm_gains, gain_part, spread, table, mix_row, w_mix, big, n_ep, n_tp
):
    seqs, width = tokens.shape
    block, part = width // n_ep, width // n_tp
    cells = spread.shape[0]
    cap = cells // n_ep
    ratio = n_ep // n_tp
    bf16, f32 = jnp.bfloat16, jnp.float32
    eff, dff = big[0].shape[1], big[3].shape[1]
    mixw = mixed.shape[1]
    rows = n_ep * seqs
    tile = 128

    def kernel(mix, tok, gains, gpart, spr, tab, mrow, wm, h0, h1, h2, h3, h4, h5, out,
               mix_all, mp, mpr, resid_at, fx, fr, ox, orr, dp, dpy, dpz, dpr, hid, ret, retr,
               dh, dha, dd, ddr, sq, sqr, wg, wu, wd, dg, du, dw, send, recv, load):
        loads = []
        for i, (h, v) in enumerate(((h3, dg), (h4, du), (h0, wg), (h1, wu), (h2, wd), (h5, dw))):
            loads.append(pltpu.make_async_copy(h, v, load.at[i]))
            loads[-1].start()

        def go(p, x, o, mode):
            return begin(p, x, o, mode, n_ep, n_tp, send, recv)

        enter("all", n_ep, n_tp)
        go(0, mix, mix_all, "bcast")()
        partial = dot32(mix_all[...].reshape(rows, mixw), wm[...]).astype(bf16)
        for e in range(n_ep):
            mp[e] = partial[e * seqs : (e + 1) * seqs]
        go(1, mp, mpr, "all")()
        pieces = []
        for e in range(n_ep):
            total = mpr[e, 0].astype(f32)
            for t in range(1, n_tp):
                total += mpr[e, t].astype(f32)
            pieces.append(total)
        mix_wide = jnp.concatenate(pieces, axis=1).astype(bf16).astype(f32)
        after = tok[...].astype(f32) + mix_wide * rms_scale(mix_wide) * gains[1:2, :]
        ffn_in = (after * rms_scale(after) * gains[2:3, :]).astype(bf16)
        for e in range(n_ep):
            fx[e] = ffn_in[:, e * block : (e + 1) * block]
        sent_dense = go(2, fx, fr, "a2a")
        outgoing = dot32(spr[...], ffn_in)
        for e in range(n_ep):
            ox[e] = outgoing[e * cap : (e + 1) * cap].astype(bf16)
        sent_routed = go(3, ox, orr, "a2a")
        for t in range(n_tp):
            resid_at[t] = after[:, t * part : (t + 1) * part]
        weight = jax.nn.sigmoid(
            jnp.sum(ffn_in.astype(f32) * mrow[...].astype(f32), axis=1, keepdims=True)
        )
        sent_dense()
        loads[0].wait()
        loads[1].wait()
        dense_rows = fr[...].reshape(rows, block)
        half = 256
        for i, w in enumerate((dg, du)):
            for c in range(0, dff, half):
                piece = dot32(dense_rows, w[:, c : c + half]).astype(bf16)
                for e in range(n_ep):
                    dp[e, :, i * dff + c : i * dff + c + half] = piece[e * seqs : (e + 1) * seqs]
        sent_pre = pair_reduce(4, 9, dp, dpy, dpz, dpr, n_ep, n_tp, send, recv)
        sent_routed()
        for wait in loads[2:]:
            wait.wait()
        expert_rows = orr[...].astype(f32).reshape(cells, width).astype(bf16)

        @pl.loop(0, eff // tile)
        def _(i):
            at = pl.ds(pl.multiple_of(i * tile, tile), tile)
            both = dot32(expert_rows, jnp.concatenate([wg[:, at], wu[:, at]], axis=1))
            hid[:, at] = (silu(both[:, :tile]) * both[:, tile:]).astype(bf16)

        @pl.loop(0, n_tp)
        def _(t):
            at = pl.ds(pl.multiple_of(t * part, part), part)
            piece = dot32(hid[...], wd[:, at])
            for e in range(n_ep):
                ret[e, t] = piece[e * cap : (e + 1) * cap].astype(bf16)

        sent_return = go(6, ret, retr, "all")
        sent_pre()
        for c in range(0, dff, half):
            gate = dpr[0, :, c : c + half].astype(f32)
            up = dpr[0, :, dff + c : dff + c + half].astype(f32)
            for e in range(1, n_ep // 2):
                gate += dpr[e, :, c : c + half].astype(f32)
                up += dpr[e, :, dff + c : dff + c + half].astype(f32)
            dh[:, c : c + half] = (silu(gate) * up).astype(bf16)
        pair_gather(5, 10, dh, dha, n_ep, n_tp, send, recv)
        partial = dot32(dha[...].reshape(rows, dff), dw[...]).astype(bf16)
        for e in range(n_ep):
            dd[e] = partial[e * seqs : (e + 1) * seqs]
        sent_out = go(7, dd, ddr, "cols")
        sent_return()
        pieces = []
        for e in range(n_ep):
            total = retr[e, 0].astype(f32)
            for t in range(1, n_tp):
                total += retr[e, t].astype(f32)
            pieces.append(total.astype(bf16).astype(f32))
        expert_sum = jnp.dot(
            tab[...],
            jnp.concatenate(pieces, axis=0),
            precision=lax.Precision.HIGHEST,
            preferred_element_type=f32,
        )
        sent_out()
        pieces = []
        for j in range(ratio):
            total = ddr[j, 0].astype(f32)
            for t in range(1, n_tp):
                total += ddr[j, t].astype(f32)
            pieces.append(total)
        ffn_out = expert_sum + weight * jnp.concatenate(pieces, axis=1)
        own = jnp.sum(ffn_out * ffn_out, axis=1, keepdims=True)
        sq[...] = jnp.broadcast_to(own, (seqs, tile))
        go(8, sq, sqr, "bcast_tp")()
        total = sqr[0]
        for t in range(1, n_tp):
            total += sqr[t]
        scale = lax.rsqrt(total[:, 0:1] / width + EPS)
        mine = resid_at[lax.axis_index("tp")]
        out[...] = (mine + ffn_out * scale * gpart[...]).astype(bf16)

    vmem = pl.BlockSpec(memory_space=pltpu.VMEM)
    hbm = pl.BlockSpec(memory_space=pl.ANY)
    b = lambda *s: pltpu.VMEM(s, bf16)
    f = lambda *s: pltpu.VMEM(s, f32)
    return pl.pallas_call(
        kernel,
        out_shape=jax.ShapeDtypeStruct((seqs, part), bf16),
        in_specs=[vmem] * 8 + [hbm] * 6,
        out_specs=vmem,
        scratch_shapes=[
            b(n_ep, seqs, mixw),
            b(n_ep, seqs, block),
            b(n_ep, n_tp, seqs, block),
            f(n_tp, seqs, part),
            b(n_ep, seqs, block),
            b(n_ep, seqs, block),
            b(n_ep, cap, width),
            b(n_ep, cap, width),
            b(n_ep, seqs, 2 * dff),
            b(n_ep // 2, seqs, 2 * dff),
            b(n_ep // 2, seqs, 2 * dff),
            b(n_ep // 2, seqs, 2 * dff),
            b(cells, eff),
            b(n_ep, n_tp, cap, part),
            b(n_ep, n_tp, cap, part),
            b(seqs, dff),
            b(n_ep, seqs, dff),
            b(n_ep, seqs, block),
            b(ratio, n_tp, seqs, block),
            f(seqs, tile),
            f(n_tp, seqs, tile),
        ]
        + [pltpu.VMEM(w.shape, bf16) for w in big]
        + [
            pltpu.SemaphoreType.DMA((11, n_ep * n_tp)),
            pltpu.SemaphoreType.DMA((11, n_ep * n_tp)),
            pltpu.SemaphoreType.DMA((6,)),
        ],
        compiler_params=pltpu.CompilerParams(
            collective_id=2, has_side_effects=True, vmem_limit_bytes=48 * 1024 * 1024
        ),
        name="finish_layer",
    )(mixed, tokens, norm_gains, gain_part, spread, table, mix_row, w_mix, *big)


def fast_body(
    tokens,
    old_state,
    lower_bound,
    head_gain,
    norm_gains,
    w_query,
    w_forget,
    w_value,
    w_outgate,
    w_mix_out,
    routes,
    route_scores,
    w_exp_gate,
    w_exp_up,
    w_exp_down,
    w_dense_gate,
    w_dense_up,
    w_dense_down,
    dense_mix,
):
    bf16, f32 = jnp.bfloat16, jnp.float32
    n_ep, n_tp = lax.axis_size("ep"), lax.axis_size("tp")
    seqs, width = tokens.shape
    part_width = width // n_tp
    projected = project(
        tokens, norm_gains, (w_query, w_forget, w_value, w_outgate), n_ep, n_tp
    )
    query_raw, forget_raw, value, out_gate = jnp.split(projected, 4, axis=1)
    heads, head_size = old_state.shape[1], old_state.shape[2]
    shape_heads = (seqs, heads, head_size)
    forget = lower_bound + (1.0 - lower_bound) * jax.nn.sigmoid(forget_raw)
    key_in = (1.0 - lower_bound) * jax.nn.sigmoid(-forget_raw)
    new_state = forget.reshape(shape_heads)[..., None] * old_state + key_in.reshape(shape_heads)[
        ..., None
    ] * value.reshape(seqs, heads, 1, head_size)
    query = jax.nn.silu(query_raw).reshape(shape_heads)
    read = jnp.sum(query[..., None] * new_state, axis=2)
    gated = (
        read
        * rms_scale(read)
        * head_gain.reshape(heads, head_size)
        * jax.nn.silu(out_gate).reshape(shape_heads)
    )
    mixed_heads = gated.reshape(seqs, heads * head_size).astype(bf16)
    topk = routes.shape[1]
    capacity = max(2, 2 * seqs * topk // n_ep)
    flat_routes = routes.reshape(-1)
    onehot = (flat_routes[:, None] == jnp.arange(n_ep, dtype=jnp.int32)[None, :]).astype(jnp.int32)
    earlier = jnp.arange(seqs * topk)[None, :] < jnp.arange(seqs * topk)[:, None]
    same = flat_routes[:, None] == flat_routes[None, :]
    slots = jnp.sum((same & earlier).astype(jnp.int32), axis=1)
    cells = flat_routes * capacity + slots
    placed = cells[None, :] == jnp.arange(n_ep * capacity, dtype=jnp.int32)[:, None]
    placed_tokens = placed.astype(bf16).reshape(n_ep * capacity, seqs, topk).sum(axis=2)
    first = jax.nn.sigmoid(route_scores[:, 0] - route_scores[:, 1])
    second = jax.nn.sigmoid(route_scores[:, 1] - route_scores[:, 0])
    route_weight = jnp.stack([first, second], axis=1).reshape(-1)
    weight_table = jnp.sum(
        (placed.astype(f32) * route_weight[None, :]).reshape(n_ep * capacity, seqs, topk), axis=2
    )
    gain_part = lax.dynamic_slice_in_dim(
        norm_gains[3:4], lax.axis_index("tp") * part_width, part_width, 1
    )
    layer_out = finish_layer(
        mixed_heads,
        tokens,
        norm_gains,
        gain_part,
        placed_tokens,
        weight_table.T,
        dense_mix[None, :],
        w_mix_out,
        (w_exp_gate[0], w_exp_up[0], w_exp_down[0], w_dense_gate, w_dense_up, w_dense_down),
        n_ep,
        n_tp,
    )
    return (layer_out, new_state)


def solution(mesh):
    n_ep, n_tp = mesh.shape['ep'], mesh.shape['tp']
    fits = n_ep % n_tp == 0 and n_ep % 2 == 0 and n_ep * n_tp <= 64
    return jax.shard_map(
        fast_body if fits else body,
        mesh=mesh,
        in_specs=(
            P("ep", None),
            P("ep", "tp", None, None),
            P("tp"),
            P("tp"),
            P(),
            P("ep", "tp"),
            P("ep", "tp"),
            P("ep", "tp"),
            P("ep", "tp"),
            P("tp", "ep"),
            P("ep", None),
            P("ep", None),
            P("ep", None, "tp"),
            P("ep", None, "tp"),
            P("ep", "tp", None),
            P("ep", "tp"),
            P("ep", "tp"),
            P("tp", "ep"),
            P(),
        ),
        out_specs=(P("ep", "tp"), P("ep", "tp", None, None)),
        check_vma=False,
    )
```

profile of v0, /device:TPU:0, one launch (start us, length us, event | category | flops | bytes accessed | tf_op | source)
XLA Modules:
  0.0 92.3 jit_solution(15305451223099073944)
XLA Ops:
  0.6 19.4 %project.1 = f32[16,2048]{1,0:T(8,128)} custom-call(bf16[16,2048]{1,0:T(8,128)(2,1)} %tok.3, f32[4,2048]{1,0:T(4,128)} %gains.3, bf16[256,512]{1,0:T(8,128)(2,1)} %w0.1, bf16[256,512]{1,0:T(8,128)(2,1)} %w1.1, bf16[256,512]{1,0:T(8,128)(2,1)} %w2.1, bf16[256,512]{1,0:T(8,128)(2,1)} %w3.1), custom_call_target="tpu_custom_call" | custom-call | tf_op jit(solution)/shard_map/project/pallas_call | solution.py:357
  20.0 0.7 broadcast_subtract_fusion
  20.7 0.8 multiply_add_fusion.1
  21.6 0.0 copy-start.8
  21.7 0.0 copy-start.5
  21.7 0.0 copy-start.9
  21.7 0.0 copy-start.7
  21.7 0.0 copy-start.6
  21.7 0.0 copy-start
  21.7 0.0 copy-start.1
  21.7 0.0 copy-start.2
  21.7 0.0 copy-start.3
  21.8 0.0 copy-start.4
  21.8 8.3 %multiply_reduce_fusion = (f32[16,4,128]{2,1,0:T(4,128)S(1)}, f32[16,4,128,128]{3,2,1,0:T(8,128)}) fusion(f32[16,4,128]{2,1,0:T(4,128)S(1)} %mul.108, f32[16,4,128]{2,1,0:T(4,128)S(1)} %mul.118, f32[16,4,128]{2,1,0:T(4,128)S(1)} %mul.116, f32[16,4,128,128]{3,2,1,0:T(8,128)} %param.20, f32[16,4,128]{2,1,0:T(4,128)S(1)} %mul.112), kind=kLoop, calls=%fused_computation | loop fusion | flops 5234688 | bytes 8552448 | tf_op jit(solution)/shard_map/reduce_sum | solution.py:585
  30.0 0.1 multiply_reduce_fusion.1
  30.1 0.1 broadcast_multiply_fusion
  30.2 0.0 copy-done.8
  30.2 0.8 fusion.1.mix
  31.0 0.0 copy-done.5
  31.1 0.0 copy-done.9
  31.1 0.0 copy-done.7
  31.1 0.1 copy.34
  31.2 0.1 eq.30
  31.3 0.2 convert_reduce_fusion
  31.5 0.1 reduce_sum.53
  31.6 0.1 copy.35
  31.7 0.1 select_reduce_fusion
  31.7 0.1 fusion.4
  31.8 0.1 copy.36.spr
  31.9 0.0 copy-done.6
  32.0 0.0 copy-done
  32.0 0.0 copy-done.1
  32.0 0.0 copy-done.2
  32.0 0.0 copy-done.3
  32.0 0.0 copy-done.4
  32.0 59.7 %finish_layer.1 = bf16[16,512]{1,0:T(8,128)(2,1)S(1)} custom-call(bf16[16,512]{1,0:T(8,128)(2,1)S(1)} %fusion.1.mix, bf16[16,2048]{1,0:T(8,128)(2,1)S(1)} %copy-done.3, f32[4,2048]{1,0:T(4,128)S(1)} %copy-done.5, f32[1,512]{1,0:T(1,128)S(1)} %constant_dynamic-slice_fusion.gpart, bf16[64,16]{1,0:T(8,128)(2,1)S(1)} %copy.36.spr, f32[16,64]{1,0:T(8,128)S(1)} %bitcast.11, ...), custom_call_target="tpu_custom_call" | custom-call | tf_op jit(solution)/shard_map/finish_layer/pallas_call | solution.py:507
  91.7 0.6 copy.40
  (11 shorter events, 0.1 us)
Async XLA Ops:
  21.6 8.6 %copy-start.8 = (f32[512]{0:T(512)S(1)}, f32[512]{0:T(512)}, u32[]{:S(2)}) copy-start(f32[512]{0:T(512)} %param.22) | copy-start | bytes 6148
  21.7 9.4 %copy-start.5 = (f32[4,2048]{1,0:T(4,128)S(1)}, f32[4,2048]{1,0:T(4,128)}, u32[]{:S(2)}) copy-start(f32[4,2048]{1,0:T(4,128)} %gains.3) | copy-start | bytes 98308
  21.7 9.4 %copy-start.9 = (f32[16,2]{0,1:T(2,128)S(1)}, f32[16,2]{0,1:T(2,128)}, u32[]{:S(2)}) copy-start(f32[16,2]{0,1:T(2,128)} %param.30) | copy-start | bytes 388
  21.7 9.4 %copy-start.7 = (s32[16,2]{0,1:T(2,128)S(1)}, s32[16,2]{0,1:T(2,128)}, u32[]{:S(2)}) copy-start(s32[16,2]{0,1:T(2,128)} %param.29) | copy-start | bytes 388
  21.7 10.2 %copy-start.6 = (bf16[2048]{0:T(1024)(128)(2,1)S(1)}, bf16[2048]{0:T(1024)(128)(2,1)}, u32[]{:S(2)}) copy-start(bf16[2048]{0:T(1024)(128)(2,1)} %param.37) | copy-start | bytes 12292
  21.7 10.2 %copy-start = (bf16[256,1536]{1,0:T(8,128)(2,1)S(1)}, bf16[256,1536]{1,0:T(8,128)(2,1)}, u32[]{:S(2)}) copy-start(bf16[256,1536]{1,0:T(8,128)(2,1)} %h3.1) | copy-start | bytes 2359300
  21.7 10.2 %copy-start.1 = (bf16[256,1536]{1,0:T(8,128)(2,1)S(1)}, bf16[256,1536]{1,0:T(8,128)(2,1)}, u32[]{:S(2)}) copy-start(bf16[256,1536]{1,0:T(8,128)(2,1)} %h4.1) | copy-start | bytes 2359300
  21.7 10.2 %copy-start.2 = (bf16[1536,256]{1,0:T(8,128)(2,1)S(1)}, bf16[1536,256]{1,0:T(8,128)(2,1)}, u32[]{:S(2)}) copy-start(bf16[1536,256]{1,0:T(8,128)(2,1)} %h5.1) | copy-start | bytes 2359300
  21.7 10.2 %copy-start.3 = (bf16[16,2048]{1,0:T(8,128)(2,1)S(1)}, bf16[16,2048]{1,0:T(8,128)(2,1)}, u32[]{:S(2)}) copy-start(bf16[16,2048]{1,0:T(8,128)(2,1)} %tok.3) | copy-start | bytes 196612
  21.8 10.2 %copy-start.4 = (bf16[512,256]{1,0:T(8,128)(2,1)S(1)}, bf16[512,256]{1,0:T(8,128)(2,1)}, u32[]{:S(2)}) copy-start(bf16[512,256]{1,0:T(8,128)(2,1)} %wm.1) | copy-start | bytes 786436
where the time goes:
time: 92.8 us; the launch traced here: 92.3 us
  Pallas kernels  79.1 us (85%)
  other arithmetic  11.1 us (12%)
  local copies, waits for them, and re-layouts  1.21 us (1%)
    pallas_call x1, Pallas kernels, finish_layer(): pl.pallas_call(kernel, out_shape=jax.ShapeDtypeStruct((seqs, part), bf16)...  59.7 us
    pallas_call x1, Pallas kernels, project(): pl.pallas_call(kernel, out_shape=jax.ShapeDtypeStruct((seqs, 4 * cols), f...  19.4 us
    reduce_sum x1, other arithmetic, fast_body(): read = jnp.sum(query[..., None] * new_state, axis=2)  8.26 us

commit v1 on v0

v1 whole, which is shorter than its diff:
```python
import jax
import jax.numpy as jnp
from jax import lax
from jax.experimental import pallas as pl
from jax.experimental.pallas import tpu as pltpu
from jax.sharding import PartitionSpec as P

EPS = 1e-06


def rms_scale(values):
    return lax.rsqrt(jnp.mean(values * values, axis=-1, keepdims=True) + EPS)


def body(
    tokens,
    old_state,
    lower_bound,
    head_gain,
    norm_gains,
    w_query,
    w_forget,
    w_value,
    w_outgate,
    w_mix_out,
    routes,
    route_scores,
    w_exp_gate,
    w_exp_up,
    w_exp_down,
    w_dense_gate,
    w_dense_up,
    w_dense_down,
    dense_mix,
):
    highest = lax.Precision.HIGHEST
    seqs, width = tokens.shape
    column_index = lax.axis_index("tp")
    part_width = width // lax.axis_size("tp")
    resid = tokens.astype(jnp.float32)
    normed = (resid * rms_scale(resid) * norm_gains[0]).astype(jnp.bfloat16)
    in_weights = jnp.concatenate([w_query, w_forget, w_value, w_outgate], axis=1)
    mix_rows = lax.all_to_all(normed, "ep", split_axis=1, concat_axis=0, tiled=True)
    projected = lax.psum_scatter(
        jnp.dot(mix_rows, in_weights, preferred_element_type=jnp.float32).astype(jnp.bfloat16),
        "ep",
        scatter_dimension=0,
        tiled=True,
    ).astype(jnp.float32)
    query_raw, forget_raw, value, out_gate = jnp.split(projected, 4, axis=1)
    heads = old_state.shape[1]
    head_size = old_state.shape[2]
    shape_heads = (seqs, heads, head_size)
    forget = lower_bound + (1.0 - lower_bound) * jax.nn.sigmoid(forget_raw)
    key_in = (1.0 - lower_bound) * jax.nn.sigmoid(-forget_raw)
    new_state = forget.reshape(shape_heads)[..., None] * old_state + key_in.reshape(shape_heads)[
        ..., None
    ] * value.reshape(seqs, heads, 1, head_size)
    query = jax.nn.silu(query_raw).reshape(shape_heads)
    read = jnp.einsum("thk,thkv->thv", query, new_state, precision=highest)
    gated = (
        read
        * rms_scale(read)
        * head_gain.reshape(heads, head_size)
        * jax.nn.silu(out_gate).reshape(shape_heads)
    )
    mixed_heads = gated.reshape(seqs, heads * head_size).astype(jnp.bfloat16)
    mix_part = jnp.dot(
        mixed_heads,
        lax.all_gather(w_mix_out, "ep", axis=1, tiled=True),
        preferred_element_type=jnp.float32,
    ).astype(jnp.bfloat16)
    mix_part = lax.optimization_barrier(mix_part).astype(jnp.float32)
    mix_out = lax.psum(mix_part.astype(jnp.bfloat16), "tp")
    mix_wide = lax.optimization_barrier(mix_out).astype(jnp.float32)
    after_mix = resid + mix_wide * rms_scale(mix_wide) * norm_gains[1]
    ffn_in = (after_mix * rms_scale(after_mix) * norm_gains[2]).astype(jnp.bfloat16)
    experts = lax.axis_size("ep")
    topk = routes.shape[1]
    capacity = max(2, 2 * seqs * topk // experts)
    flat_routes = routes.reshape(-1)
    onehot = (flat_routes[:, None] == jnp.arange(experts, dtype=jnp.int32)[None, :]).astype(
        jnp.int32
    )
    before = jnp.cumsum(onehot, axis=0) - onehot
    slots = jnp.sum(onehot * before, axis=1)
    cells = flat_routes * capacity + slots
    placed = cells[None, :] == jnp.arange(experts * capacity, dtype=jnp.int32)[:, None]
    repeated = jnp.repeat(ffn_in, topk, axis=0)
    outgoing = jnp.dot(placed.astype(jnp.bfloat16), repeated, preferred_element_type=jnp.float32)
    outgoing = outgoing.astype(jnp.bfloat16).reshape(experts, capacity, width)
    arrived = lax.all_to_all(outgoing, "ep", split_axis=0, concat_axis=0, tiled=True)
    sources, items, _ = arrived.shape
    expert_rows = arrived.reshape(sources * items, width)
    gate_pre = jnp.dot(expert_rows, w_exp_gate[0], preferred_element_type=jnp.float32)
    up_pre = jnp.dot(expert_rows, w_exp_up[0], preferred_element_type=jnp.float32)
    hidden = (jax.nn.silu(gate_pre) * up_pre).astype(jnp.bfloat16)
    partial_rows = jnp.dot(hidden, w_exp_down[0], preferred_element_type=jnp.float32).astype(
        jnp.bfloat16
    )
    partial_rows = lax.optimization_barrier(partial_rows).astype(jnp.float32)
    partial_rows = partial_rows.reshape(sources, items, width)
    summed = lax.psum_scatter(
        partial_rows.astype(jnp.bfloat16), "tp", scatter_dimension=2, tiled=True
    )
    returned = lax.all_to_all(summed, "ep", split_axis=0, concat_axis=0, tiled=True)
    first = jax.nn.sigmoid(route_scores[:, 0] - route_scores[:, 1])
    second = jax.nn.sigmoid(route_scores[:, 1] - route_scores[:, 0])
    route_weight = jnp.stack([first, second], axis=1).reshape(-1)
    weight_table = jnp.sum(
        (placed.astype(jnp.float32) * route_weight[None, :]).reshape(
            experts * capacity, seqs, topk
        ),
        axis=2,
    )
    expert_sum = jnp.dot(
        weight_table.T,
        returned.reshape(experts * capacity, part_width).astype(jnp.float32),
        precision=highest,
    )
    dense_weights = jnp.concatenate([w_dense_gate, w_dense_up], axis=1)
    dense_rows = lax.all_to_all(ffn_in, "ep", split_axis=1, concat_axis=0, tiled=True)
    dense_pre = lax.psum_scatter(
        jnp.dot(dense_rows, dense_weights, preferred_element_type=jnp.float32).astype(jnp.bfloat16),
        "ep",
        scatter_dimension=0,
        tiled=True,
    ).astype(jnp.float32)
    dense_gate_pre, dense_up_pre = jnp.split(dense_pre, 2, axis=1)
    dense_hidden = (jax.nn.silu(dense_gate_pre) * dense_up_pre).astype(jnp.bfloat16)
    dense_partial = jnp.dot(
        dense_hidden,
        lax.all_gather(w_dense_down, "ep", axis=1, tiled=True),
        preferred_element_type=jnp.float32,
    )
    dense_out = lax.psum_scatter(
        dense_partial.astype(jnp.bfloat16), "tp", scatter_dimension=1, tiled=True
    ).astype(jnp.float32)
    mix_weight = jax.nn.sigmoid(jnp.dot(ffn_in, dense_mix, preferred_element_type=jnp.float32))
    ffn_out = expert_sum + mix_weight[:, None] * dense_out
    squares = lax.psum(jnp.sum(ffn_out * ffn_out, axis=1), "tp")
    out_scale = lax.rsqrt(squares / width + EPS)
    gain_part = lax.dynamic_slice_in_dim(norm_gains[3], column_index * part_width, part_width, 0)
    resid_part = lax.dynamic_slice_in_dim(after_mix, column_index * part_width, part_width, 1)
    layer_out = (resid_part + ffn_out * out_scale[:, None] * gain_part).astype(jnp.bfloat16)
    return (layer_out, new_state)


def dot32(a, b):
    return jnp.dot(a, b, preferred_element_type=jnp.float32)


def silu(x):
    return x * jax.nn.sigmoid(x)


MESH = pl.DeviceIdType.MESH


class Sems:
    def __init__(self):
        self.used = 0

    def take(self, count):
        first = self.used
        self.used += count
        return first


def chips_by_distance(q, half):
    if half == 4:
        return [q, q + 1 - 2 * lax.rem(q, 2), 2 - q // 2, 3 - 3 * (q // 2)]
    return [q] + [lax.rem(q + k, half) for k in range(1, half)]


CHUNKS = 2


def fused_layer(
    tokens,
    old_state,
    bounds,
    head_gain,
    norm_gains,
    in_weights,
    w_mix,
    routes,
    scores,
    experts,
    dense,
    mix_row,
    n_ep,
    n_tp,
):
    bf16, f32, i32 = jnp.bfloat16, jnp.float32, jnp.int32
    seqs, width = tokens.shape
    heads, hs = old_state.shape[1:3]
    block, part = width // n_ep, width // n_tp
    chans = heads * hs
    topk = routes.shape[1]
    cap = max(2, 2 * seqs * topk // n_ep)
    cells, rows = n_ep * cap, n_ep * seqs
    eff, dff = experts[0].shape[2], dense[0].shape[1]
    half, ratio = n_ep // 2, n_ep // n_tp
    duo = 2 * seqs
    lanes = 128
    tile = 128
    chunk = dff // CHUNKS

    send_at, recv_at = Sems(), Sems()

    def pair(count):
        return send_at.take(count), recv_at.take(count)

    P_TOK, P_ROUTE = pair(n_ep), pair(n_ep)
    P_PAIR, P_HEAD = pair(heads), pair(heads * half)
    P_MIX = pair(heads * n_ep)
    P_TP = pair(half * n_tp)
    P_STAT, P_OWN = pair(n_ep), pair(n_ep)
    P_DPAIR, P_DENSE = pair(CHUNKS), pair(CHUNKS * half)
    P_EXP = pair(n_ep)
    P_RTP, P_RET = pair(n_tp), pair(n_ep)
    P_GATH, P_HAND = pair(CHUNKS * (half + 1)), pair(CHUNKS * (half + 1))
    P_COLS = send_at.take(n_ep), recv_at.take(ratio * n_tp)
    P_SQ = pair(n_tp)
    n_load = 16 + 4 * heads + 2 * CHUNKS + 2 * (eff // tile)

    def kernel(
        tok_h, st_h, lb_h, hg_h, gn_h, wq_h, wf_h, wv_h, wo_h, wm_h, rt_h, sc_h,
        eg_h, eu_h, ed_h, dg_h, du_h, dd_h, mr_h,
        out, ns,
        tok, st, lb, hg, gn, win, wm, rt0, sc, wgu, wed, wd, wdd, mrow,
        R, RT, X, Y, Z, PR, rd, MA, TX, TR, MV, STAT, SX, SR, COL, OWN, SEL, MO, MR,
        DX, DY, DZ, DR, DH, OX, ER, hid, RX, RR, RB, RG, dd, ddr, sq, sqr,
        send, recv, lsem,
    ):
        me_e, me_t = lax.axis_index("ep"), lax.axis_index("tp")
        q, c = me_e // 2, lax.rem(me_e, 2)
        partner = 2 * q + 1 - c
        chips = chips_by_distance(q, half)
        away = chips[:0:-1]
        ep_peers = [(de, lax.rem(me_e + de, n_ep)) for de in range(1, n_ep)]
        tp_peers = [(dt, lax.rem(me_t + dt, n_tp)) for dt in range(1, n_tp)]

        barrier = pltpu.get_barrier_semaphore()
        for _, e in ep_peers:
            pl.semaphore_signal(barrier, inc=1, device_id=(e, me_t), device_id_type=MESH)
        for _, t in tp_peers:
            pl.semaphore_signal(barrier, inc=1, device_id=(me_e, t), device_id_type=MESH)

        count = [0]

        def load(src, dst):
            copy = pltpu.make_async_copy(src, dst, lsem.at[count[0]])
            count[0] += 1
            copy.start()
            return copy

        l_tok = load(tok_h, tok)
        l_gn = load(gn_h, gn)
        l_rt = load(rt_h, rt0)
        l_in = [
            [
                load(w.at[:, h * hs : (h + 1) * hs], win.at[h, :, i * hs : (i + 1) * hs])
                for i, w in enumerate((wq_h, wf_h, wv_h, wo_h))
            ]
            for h in range(heads)
        ]
        l_small = [load(lb_h, lb), load(hg_h, hg), load(sc_h, sc), load(mr_h, mrow)]
        l_st = load(st_h, st)
        l_wm = load(wm_h, wm)
        l_wd = [
            [
                load(w.at[:, j * chunk : (j + 1) * chunk], wd.at[j, :, i * chunk : (i + 1) * chunk])
                for i, w in enumerate((dg_h, du_h))
            ]
            for j in range(CHUNKS)
        ]
        l_exp = []
        for i in range(eff // tile):
            for k, w in enumerate((eg_h, eu_h)):
                at = (2 * i + k) * tile
                l_exp.append(load(w.at[0, :, i * tile : (i + 1) * tile], wgu.at[:, at : at + tile]))
        l_exp.append(load(ed_h.at[0], wed))
        l_wdd = load(dd_h, wdd)

        sent = []

        def put(src, dst, device, s, r):
            copy = pltpu.make_async_remote_copy(
                src_ref=src,
                dst_ref=dst,
                send_sem=send.at[s],
                recv_sem=recv.at[r],
                device_id=device,
                device_id_type=MESH,
            )
            copy.start()
            sent.append(copy.wait_send)

        def arrive(like, dst, r):
            pltpu.make_async_copy(like, dst, recv.at[r]).wait()

        def cut(first, size):
            return pl.ds(pl.multiple_of(first, 128), size)

        mine = cut(me_e * block, block)
        own_rows = pl.ds(pl.multiple_of(me_e * seqs, seqs), seqs)

        l_tok.wait()
        l_gn.wait()
        l_rt.wait()
        pl.semaphore_wait(barrier, n_ep + n_tp - 2)
        for de, e in ep_peers:
            put(tok.at[:, cut(e * block, block)], R.at[me_e], (e, me_t), P_TOK[0] + de, P_TOK[1] + de)
        for de, e in ep_peers:
            put(rt0, RT.at[me_e], (e, me_t), P_ROUTE[0] + de, P_ROUTE[1] + de)
        R[me_e] = tok[:, mine]
        RT[me_e] = rt0[...]
        resid = tok[...].astype(f32)
        scale0 = rms_scale(resid)
        g0 = gn[0:1, mine]
        g1 = gn[1:2, mine]
        g2 = gn[2:3, mine]
        for group in l_in:
            for copy in group:
                copy.wait()
        for de, _ in ep_peers:
            arrive(rt0, RT.at[0], P_ROUTE[1] + de)
            arrive(tok.at[:, 0:block], R.at[0], P_TOK[1] + de)

        scaled = (R[...].reshape(rows, block).astype(f32) * g0).astype(bf16)
        for h in range(heads):
            piece = dot32(scaled, win[h]).astype(bf16)
            for e in range(n_ep):
                X[h, e % 2, e // 2] = piece[e * seqs : (e + 1) * seqs]
            put(X.at[h, 1 - c], Y.at[h], (partner, me_t), P_PAIR[0] + h, P_PAIR[1] + h)
        for h in range(heads):
            arrive(X.at[h, 0], Y.at[h], P_PAIR[1] + h)
            for k, kk in enumerate(away):
                Z[h, kk] = (X[h, c, kk].astype(f32) + Y[h, kk].astype(f32)).astype(bf16)
                put(
                    Z.at[h, kk],
                    PR.at[h, q],
                    (2 * kk + c, me_t),
                    P_HEAD[0] + h * half + k,
                    P_HEAD[1] + h * half + q,
                )
            PR[h, q] = (X[h, c, q].astype(f32) + Y[h, q].astype(f32)).astype(bf16)

        named = RT[...].reshape(rows, topk)
        lane = lax.broadcasted_iota(i32, (rows, lanes), 1)
        row = lax.broadcasted_iota(i32, (rows, lanes), 0)
        ones = [(lane == named[:, k : k + 1]).astype(f32) for k in range(topk)]
        earlier = ((lane < row) & (lane >= (row // seqs) * seqs)).astype(bf16)
        before = dot32(earlier, sum(ones).astype(bf16))
        slots = [
            jnp.sum(o * before, axis=1, keepdims=True).astype(i32) for o in ones
        ]
        spot = lax.broadcasted_iota(i32, (rows, 1), 0) // seqs
        wide = lax.broadcasted_iota(i32, (rows, n_ep * cells), 1)
        chosen = jnp.zeros((rows, n_ep * cells), f32)
        for k in range(topk):
            place = named[:, k : k + 1] * cells + spot * cap + slots[k]
            chosen = chosen + (wide == place).astype(f32)
        for i in range(n_ep * cells // lanes):
            SEL[i * lanes : (i + 1) * lanes, :] = chosen[:, i * lanes : (i + 1) * lanes].T.astype(bf16)
        ours = jnp.zeros((rows, lanes), i32)
        for k in range(topk):
            ours = ours + jnp.where(lane == k, named[:, k : k + 1] * cap + slots[k], 0)
        OWN[...] = ours
        for copy in l_small:
            copy.wait()
        at_own = OWN[own_rows, :]
        spread = lax.broadcasted_iota(i32, (seqs, cells), 1)
        gap = sc[:, 0:1] - sc[:, 1:2]
        table = jnp.where(spread == at_own[:, 0:1], jax.nn.sigmoid(gap), 0.0)
        table = table + jnp.where(spread == at_own[:, 1:2], jax.nn.sigmoid(-gap), 0.0)

        l_st.wait()
        for h in range(heads):
            for kk in chips[1:]:
                arrive(Z.at[h, 0], PR.at[h, 0], P_HEAD[1] + h * half + kk)
            total = PR[h, 0].astype(f32)
            for kk in range(1, half):
                total = total + PR[h, kk].astype(f32)
            total = total * scale0
            at = slice(h * hs, (h + 1) * hs)
            bound = lb[0:1, at]
            raw = total[:, hs : 2 * hs]
            forget = bound + (1.0 - bound) * jax.nn.sigmoid(raw)
            key_in = (1.0 - bound) * jax.nn.sigmoid(-raw)
            query = silu(total[:, 0:hs])
            value = total[:, 2 * hs : 3 * hs]
            columns = jnp.concatenate(
                [forget, key_in, query, jnp.zeros((hs - 3 * seqs, hs), f32)], axis=0
            ).T
            for s in range(seqs):
                new = (
                    columns[:, s : s + 1] * st[s, h]
                    + columns[:, seqs + s : seqs + s + 1] * value[s : s + 1, :]
                )
                ns[s, h] = new
                rd[s : s + 1, :] = jnp.sum(
                    columns[:, 2 * seqs + s : 2 * seqs + s + 1] * new, axis=0, keepdims=True
                )
            read = rd[...]
            gated = read * rms_scale(read) * hg[0:1, at] * silu(total[:, 3 * hs :])
            MA[h, me_e] = gated.astype(bf16)
            for de, e in ep_peers:
                put(
                    MA.at[h, me_e],
                    MA.at[h, me_e],
                    (e, me_t),
                    P_MIX[0] + h * n_ep + de,
                    P_MIX[1] + h * n_ep + me_e,
                )

        l_wm.wait()
        for g, kk in enumerate(chips):
            for e in (2 * kk, 2 * kk + 1):
                if g == 0:
                    continue
                for h in range(heads):
                    arrive(MA.at[h, 0], MA.at[h, 1], P_MIX[1] + h * n_ep + e)
            if g == 0:
                for h in range(heads):
                    arrive(MA.at[h, 0], MA.at[h, 1], P_MIX[1] + h * n_ep + partner)
            lhs = jnp.concatenate(
                [MA[h, pl.ds(2 * kk, 2)].reshape(duo, hs) for h in range(heads)], axis=1
            )
            piece = dot32(lhs, wm[...]).astype(bf16)
            TX[kk] = piece
            TR[me_t, kk] = piece
            for dt, t in tp_peers:
                put(
                    TX.at[kk],
                    TR.at[me_t, kk],
                    (me_e, t),
                    P_TP[0] + g * n_tp + dt,
                    P_TP[1] + kk * n_tp + me_t,
                )
        lane_duo = lax.broadcasted_iota(i32, (duo, lanes), 1)
        mixer = mrow[0:1, mine].astype(f32)
        for kk in chips:
            for _, t in tp_peers:
                arrive(TX.at[0], TR.at[0, 0], P_TP[1] + kk * n_tp + t)
            total = TR[0, kk].astype(f32)
            for t in range(1, n_tp):
                total = total + TR[t, kk].astype(f32)
            narrow = total.astype(bf16)
            MO[pl.ds(2 * kk, 2)] = narrow.reshape(2, seqs, block)
            mixed = narrow.astype(f32)
            MV[kk] = mixed
            base = R[pl.ds(2 * kk, 2)].reshape(duo, block).astype(f32)
            lifted = mixed * g1
            figures = (
                base * base,
                mixed * mixed,
                base * lifted,
                lifted * lifted,
                base * g2 * mixer,
                lifted * g2 * mixer,
            )
            stat = jnp.zeros((duo, lanes), f32)
            for i, figure in enumerate(figures):
                stat = stat + jnp.where(
                    lane_duo == i, jnp.sum(figure, axis=1, keepdims=True), 0.0
                )
            STAT[kk] = stat
        SX[...] = STAT[...].reshape(rows, lanes).T[0:8, :]
        SR[me_e] = SX[...]
        for de, e in ep_peers:
            put(SX, SR.at[me_e], (e, me_t), P_STAT[0] + de, P_STAT[1] + de)

        def send_own():
            for de, e in ep_peers:
                pltpu.make_async_remote_copy(
                    src_ref=MO.at[e],
                    dst_ref=MR.at[lax.rem(me_e, ratio)],
                    send_sem=send.at[P_OWN[0] + de],
                    recv_sem=recv.at[P_OWN[1] + lax.rem(me_e, ratio)],
                    device_id=(e, me_t),
                    device_id_type=MESH,
                ).start()
            MR[lax.rem(me_e, ratio)] = MO[me_e]

        def sent_own():
            for de, e in ep_peers:
                pltpu.make_async_remote_copy(
                    src_ref=MO.at[e],
                    dst_ref=MR.at[lax.rem(me_e, ratio)],
                    send_sem=send.at[P_OWN[0] + de],
                    recv_sem=recv.at[P_OWN[1] + lax.rem(me_e, ratio)],
                    device_id=(e, me_t),
                    device_id_type=MESH,
                ).wait_send()

        holds = me_e // ratio == me_t
        pl.when(holds)(send_own)

        for de, _ in ep_peers:
            arrive(SX, SR.at[0], P_STAT[1] + de)
        total = SR[0]
        for e in range(1, n_ep):
            total = total + SR[e]
        inv_mix = lax.rsqrt(total[1:2] / width + EPS)
        squares = total[0:1] + 2.0 * inv_mix * total[2:3] + inv_mix * inv_mix * total[3:4]
        inv_after = lax.rsqrt(jnp.maximum(squares, 0.0) / width + EPS)
        weight = jax.nn.sigmoid(inv_after * (total[4:5] + inv_mix * total[5:6]))
        back = jnp.where(row == 0, inv_mix, jnp.where(row == 1, inv_after, jnp.where(row == 2, weight, 0.0)))
        back = back.T
        COL[...] = back
        after = R[...].reshape(rows, block).astype(f32) + MV[...].reshape(rows, block) * back[:, 0:1] * g1
        ffn_in = (after * back[:, 1:2] * g2).astype(bf16)

        step = 256
        for j in range(CHUNKS):
            for copy in l_wd[j]:
                copy.wait()
            for a in range(0, 2 * chunk, step):
                piece = dot32(ffn_in, wd[j, :, a : a + step]).astype(bf16)
                for e in range(n_ep):
                    DX[j, e % 2, e // 2, :, a : a + step] = piece[e * seqs : (e + 1) * seqs]
            put(DX.at[j, 1 - c], DY.at[j], (partner, me_t), P_DPAIR[0] + j, P_DPAIR[1] + j)
            if j == 0:
                routed = dot32(SEL[...], ffn_in).astype(bf16)
                for e in range(n_ep):
                    OX[e] = routed[e * cells : (e + 1) * cells]
                for de, e in ep_peers:
                    put(OX.at[e], ER.at[:, mine], (e, me_t), P_EXP[0] + de, P_EXP[1] + de)
                ER[:, mine] = OX[me_e]
        for j in range(CHUNKS):
            arrive(DX.at[j, 0], DY.at[j], P_DPAIR[1] + j)
            for k, kk in enumerate(away):
                DZ[j, kk] = (DX[j, c, kk].astype(f32) + DY[j, kk].astype(f32)).astype(bf16)
                put(
                    DZ.at[j, kk],
                    DR.at[j, q],
                    (2 * kk + c, me_t),
                    P_DENSE[0] + j * half + k,
                    P_DENSE[1] + j * half + q,
                )
            DR[j, q] = (DX[j, c, q].astype(f32) + DY[j, q].astype(f32)).astype(bf16)

        for copy in l_exp:
            copy.wait()
        for de, _ in ep_peers:
            arrive(OX.at[0], ER.at[:, 0:block], P_EXP[1] + de)

        @pl.loop(0, eff // tile)
        def _(i):
            both = dot32(ER[...], wgu[:, cut(i * 2 * tile, 2 * tile)])
            hid[:, cut(i * tile, tile)] = (silu(both[:, :tile]) * both[:, tile:]).astype(bf16)

        for dt, t in tp_peers + [(0, me_t)]:
            piece = dot32(hid[...], wed[:, cut(t * part, part)]).astype(bf16)
            if dt:
                RX[dt] = piece
                put(RX.at[dt], RR.at[me_t], (me_e, t), P_RTP[0] + dt, P_RTP[1] + dt)
            else:
                RR[me_t] = piece

        def hidden(j):
            for kk in chips[1:]:
                arrive(DZ.at[j, 0], DR.at[j, 0], P_DENSE[1] + j * half + kk)
            for a in range(0, chunk, step):
                gate = DR[j, 0, :, a : a + step].astype(f32)
                up = DR[j, 0, :, chunk + a : chunk + a + step].astype(f32)
                for kk in range(1, half):
                    gate = gate + DR[j, kk, :, a : a + step].astype(f32)
                    up = up + DR[j, kk, :, chunk + a : chunk + a + step].astype(f32)
                DH[j, me_e, :, a : a + step] = (silu(gate) * up).astype(bf16)
            base = j * (half + 1)
            for k, kk in enumerate(away):
                put(
                    DH.at[j, me_e],
                    DH.at[j, me_e],
                    (2 * kk + c, me_t),
                    P_GATH[0] + base + k,
                    P_GATH[1] + base + q,
                )
            put(
                DH.at[j, me_e],
                DH.at[j, me_e],
                (partner, me_t),
                P_GATH[0] + base + half,
                P_GATH[1] + base + half,
            )

        def hand_over(j):
            base = j * (half + 1)
            for k, kk in enumerate(chips[1:]):
                arrive(DH.at[j, 0], DH.at[j, 1], P_GATH[1] + base + kk)
                here = DH.at[j, 2 * kk + c]
                put(here, here, (partner, me_t), P_HAND[0] + base + k, P_HAND[1] + base + kk)

        def gathered(j):
            base = j * (half + 1)
            arrive(DH.at[j, 0], DH.at[j, 1], P_GATH[1] + base + half)
            for kk in chips[1:]:
                arrive(DH.at[j, 0], DH.at[j, 1], P_HAND[1] + base + kk)
            return dot32(DH[j].reshape(rows, chunk), wdd[j * chunk : (j + 1) * chunk, :])

        def give_back():
            for dt, _ in tp_peers:
                arrive(RX.at[0], RR.at[0], P_RTP[1] + dt)
            total = RR[0].astype(f32)
            for t in range(1, n_tp):
                total = total + RR[t].astype(f32)
            total = total.astype(bf16)
            for e in range(n_ep):
                RB[e] = total[e * cap : (e + 1) * cap]
            RG[me_e] = RB[me_e]
            for de, e in ep_peers:
                put(RB.at[e], RG.at[me_e], (e, me_t), P_RET[0] + de, P_RET[1] + de)

        hidden(0)
        give_back()
        for j in range(1, CHUNKS):
            hidden(j)
        for j in range(CHUNKS):
            hand_over(j)
        l_wdd.wait()
        total = gathered(0)
        for j in range(1, CHUNKS):
            total = total + gathered(j)
        total = total.astype(bf16)
        for e in range(n_ep):
            dd[e] = total[e * seqs : (e + 1) * seqs]
        to = me_e // ratio
        slot = lax.rem(me_e, ratio) * n_tp + me_t
        landing = ddr.at[lax.rem(me_e, ratio), me_t]
        for de in range(n_ep):
            e = lax.rem(me_e + de, n_ep)
            remote = pltpu.make_async_remote_copy(
                src_ref=dd.at[e],
                dst_ref=landing,
                send_sem=send.at[P_COLS[0] + de],
                recv_sem=recv.at[P_COLS[1] + slot],
                device_id=(e, to),
                device_id_type=MESH,
            )
            if de == 0:
                own = pltpu.make_async_copy(dd.at[e], landing, recv.at[P_COLS[1] + slot])
                pl.when(to == me_t)(own.start)
                pl.when(to != me_t)(remote.start)
                sent.append(lambda remote=remote: pl.when(to != me_t)(remote.wait_send))
            else:
                remote.start()
                sent.append(remote.wait_send)

        for de, _ in ep_peers:
            arrive(RB.at[0], RG.at[0], P_RET[1] + de)
        expert_sum = jnp.dot(
            table,
            RG[...].astype(f32).reshape(cells, part),
            precision=lax.Precision.HIGHEST,
            preferred_element_type=f32,
        )
        own_cols = COL[own_rows, :]
        part_at = cut(me_t * part, part)
        for j in range(ratio):
            source = me_t * ratio + j

            def wait_own(j=j):
                arrive(MO.at[0], MR.at[j], P_OWN[1] + j)

            pl.when(source != me_e)(wait_own)
        mix_own = jnp.concatenate([MR[j].astype(f32) for j in range(ratio)], axis=1)
        after_own = tok[:, part_at].astype(f32) + mix_own * own_cols[:, 0:1] * gn[1:2, part_at]
        for i in range(ratio * n_tp):
            arrive(dd.at[0], ddr.at[i // n_tp, i % n_tp], P_COLS[1] + i)
        pieces = []
        for j in range(ratio):
            total = ddr[j, 0].astype(f32)
            for t in range(1, n_tp):
                total = total + ddr[j, t].astype(f32)
            pieces.append(total)
        ffn_out = expert_sum + own_cols[:, 2:3] * jnp.concatenate(pieces, axis=1)
        mass = jnp.sum(ffn_out * ffn_out, axis=1, keepdims=True)
        sq[...] = jnp.broadcast_to(mass, (seqs, lanes))
        sqr[me_t] = sq[...]
        for dt, t in tp_peers:
            put(sq, sqr.at[me_t], (me_e, t), P_SQ[0] + dt, P_SQ[1] + dt)
        for dt, _ in tp_peers:
            arrive(sq, sqr.at[0], P_SQ[1] + dt)
        total = sqr[0]
        for t in range(1, n_tp):
            total = total + sqr[t]
        scale = lax.rsqrt(total[:, 0:1] / width + EPS)
        out[...] = (after_own + ffn_out * scale * gn[3:4, part_at]).astype(bf16)
        pl.when(holds)(sent_own)
        for wait in sent:
            wait()

    vmem = pl.BlockSpec(memory_space=pltpu.VMEM)
    hbm = pl.BlockSpec(memory_space=pltpu.HBM)
    b = lambda *s: pltpu.VMEM(s, bf16)
    f = lambda *s: pltpu.VMEM(s, f32)
    n = lambda *s: pltpu.VMEM(s, i32)
    return pl.pallas_call(
        kernel,
        out_shape=(
            jax.ShapeDtypeStruct((seqs, part), bf16),
            jax.ShapeDtypeStruct(old_state.shape, f32),
        ),
        in_specs=[hbm] * 19,
        out_specs=(vmem, vmem),
        scratch_shapes=[
            b(seqs, width),
            f(*old_state.shape),
            f(1, chans),
            f(1, chans),
            f(*norm_gains.shape),
            b(heads, block, 4 * hs),
            b(chans, block),
            n(seqs, topk),
            f(seqs, topk),
            b(width, 2 * eff),
            b(eff, width),
            b(CHUNKS, block, 2 * chunk),
            b(dff, block),
            b(1, width),
            b(n_ep, seqs, block),
            n(n_ep, seqs, topk),
            b(heads, 2, half, seqs, 4 * hs),
            b(heads, half, seqs, 4 * hs),
            b(heads, half, seqs, 4 * hs),
            b(heads, half, seqs, 4 * hs),
            f(seqs, hs),
            b(heads, n_ep, seqs, hs),
            b(half, duo, block),
            b(n_tp, half, duo, block),
            f(half, duo, block),
            f(half, duo, lanes),
            f(8, lanes),
            f(n_ep, 8, lanes),
            f(rows, lanes),
            n(rows, lanes),
            b(n_ep * cells, rows),
            b(n_ep, seqs, block),
            b(ratio, seqs, block),
            b(CHUNKS, 2, half, seqs, 2 * chunk),
            b(CHUNKS, half, seqs, 2 * chunk),
            b(CHUNKS, half, seqs, 2 * chunk),
            b(CHUNKS, half, seqs, 2 * chunk),
            b(CHUNKS, n_ep, seqs, chunk),
            b(n_ep, cells, block),
            b(cells, width),
            b(cells, eff),
            b(n_tp, cells, part),
            b(n_tp, cells, part),
            b(n_ep, cap, part),
            b(n_ep, cap, part),
            b(n_ep, seqs, block),
            b(ratio, n_tp, seqs, block),
            f(seqs, lanes),
            f(n_tp, seqs, lanes),
            pltpu.SemaphoreType.DMA((send_at.used,)),
            pltpu.SemaphoreType.DMA((recv_at.used,)),
            pltpu.SemaphoreType.DMA((n_load,)),
        ],
        compiler_params=pltpu.CompilerParams(
            collective_id=1, has_side_effects=True, vmem_limit_bytes=48 * 1024 * 1024
        ),
        name="fused_layer",
    )(
        tokens,
        old_state,
        bounds,
        head_gain,
        norm_gains,
        *in_weights,
        w_mix,
        routes,
        scores,
        *experts,
        *dense,
        mix_row,
    )


def fast_body(
    tokens,
    old_state,
    lower_bound,
    head_gain,
    norm_gains,
    w_query,
    w_forget,
    w_value,
    w_outgate,
    w_mix_out,
    routes,
    route_scores,
    w_exp_gate,
    w_exp_up,
    w_exp_down,
    w_dense_gate,
    w_dense_up,
    w_dense_down,
    dense_mix,
):
    return fused_layer(
        tokens,
        old_state,
        lower_bound[None, :],
        head_gain[None, :],
        norm_gains,
        (w_query, w_forget, w_value, w_outgate),
        w_mix_out,
        routes,
        route_scores,
        (w_exp_gate, w_exp_up, w_exp_down),
        (w_dense_gate, w_dense_up, w_dense_down),
        dense_mix[None, :],
        lax.axis_size("ep"),
        lax.axis_size("tp"),
    )


def solution(mesh):
    n_ep, n_tp = mesh.shape['ep'], mesh.shape['tp']
    fits = n_ep % n_tp == 0 and n_ep % 2 == 0 and n_ep * n_tp <= 64
    return jax.shard_map(
        fast_body if fits else body,
        mesh=mesh,
        in_specs=(
            P("ep", None),
            P("ep", "tp", None, None),
            P("tp"),
            P("tp"),
            P(),
            P("ep", "tp"),
            P("ep", "tp"),
            P("ep", "tp"),
            P("ep", "tp"),
            P("tp", "ep"),
            P("ep", None),
            P("ep", None),
            P("ep", None, "tp"),
            P("ep", None, "tp"),
            P("ep", "tp", None),
            P("ep", "tp"),
            P("ep", "tp"),
            P("tp", "ep"),
            P(),
        ),
        out_specs=(P("ep", "tp"), P("ep", "tp", None, None)),
        check_vma=False,
    )
```

time: 92.8 us -> 89 us (0.959)
  local copies, waits for them, and re-layouts: 1.21 us -> 18.6 us
  other arithmetic: 11.1 us -> 0 us
  Pallas kernels: 79.1 us -> 69 us
    unnamed x22 -> x28, local copies, waits for them, and re-layouts: 0.75 us -> 17.9 us
    pallas_call x2 -> x1, Pallas kernels: 79.1 us -> 69 us  [fused_layer(): pl.pallas_call(kernel, out_shape=(jax.ShapeDtypeStruct((seqs, part), bf16...]
    reduce_sum x5 -> x0, other arithmetic: 8.69 us -> none  [the longest x1 8.26 us: fast_body(): read = jnp.sum(query[..., None] * new_state, axis=2)]
where the time goes in v1:
time: 89 us; the launch traced here: 88.3 us
  Pallas kernels  69 us (78%)
  local copies, waits for them, and re-layouts  18.6 us (21%)
    pallas_call x1, Pallas kernels, fused_layer(): pl.pallas_call(kernel, out_shape=(jax.ShapeDtypeStruct((seqs, part), bf16...  69 us
    unnamed x28, local copies, waits for them, and re-layouts  17.9 us

profile of v1, /device:TPU:0, one launch (start us, length us, event | category | flops | bytes accessed | tf_op | source)
XLA Modules:
  0.0 88.3 jit_solution(7386755362620628294)
XLA Ops:
  0.6 0.8 copy.21.rt_h
  1.4 0.8 copy.22.sc_h
  2.1 0.7 broadcast_in_dim.11.mr_h
  2.8 0.0 copy-start
  2.8 1.1 %copy-done = bf16[256,1536]{1,0:T(8,128)(2,1)S(1)} copy-done((bf16[256,1536]{1,0:T(8,128)(2,1)S(1)}, bf16[256,1536]{1,0:T(8,128)(2,1)}, u32[]{:S(2)}) %copy-start) | copy-done | bytes 786456
  4.0 0.0 copy-start.1
  4.0 1.1 %copy-done.1 = bf16[256,1536]{1,0:T(8,128)(2,1)S(1)} copy-done((bf16[256,1536]{1,0:T(8,128)(2,1)S(1)}, bf16[256,1536]{1,0:T(8,128)(2,1)}, u32[]{:S(2)}) %copy-start.1) | copy-done | bytes 786456
  5.1 0.0 copy-start.2
  5.1 1.1 %copy-done.2 = bf16[1536,256]{1,0:T(8,128)(2,1)S(1)} copy-done((bf16[1536,256]{1,0:T(8,128)(2,1)S(1)}, bf16[1536,256]{1,0:T(8,128)(2,1)}, u32[]{:S(2)}) %copy-start.2) | copy-done | bytes 786456
  6.2 0.0 copy-start.3
  6.2 0.9 %copy-done.3 = bf16[256,512]{1,0:T(8,128)(2,1)S(1)} copy-done((bf16[256,512]{1,0:T(8,128)(2,1)S(1)}, bf16[256,512]{1,0:T(8,128)(2,1)}, u32[]{:S(2)}) %copy-start.3) | copy-done | bytes 262168
  7.2 0.0 copy-start.4
  7.2 0.9 %copy-done.4 = bf16[256,512]{1,0:T(8,128)(2,1)S(1)} copy-done((bf16[256,512]{1,0:T(8,128)(2,1)S(1)}, bf16[256,512]{1,0:T(8,128)(2,1)}, u32[]{:S(2)}) %copy-start.4) | copy-done | bytes 262168
  8.1 0.0 copy-start.5
  8.1 0.9 %copy-done.5 = bf16[256,512]{1,0:T(8,128)(2,1)S(1)} copy-done((bf16[256,512]{1,0:T(8,128)(2,1)S(1)}, bf16[256,512]{1,0:T(8,128)(2,1)}, u32[]{:S(2)}) %copy-start.5) | copy-done | bytes 262168
  9.1 0.0 copy-start.6
  9.1 0.9 %copy-done.6 = bf16[256,512]{1,0:T(8,128)(2,1)S(1)} copy-done((bf16[256,512]{1,0:T(8,128)(2,1)S(1)}, bf16[256,512]{1,0:T(8,128)(2,1)}, u32[]{:S(2)}) %copy-start.6) | copy-done | bytes 262168
  10.0 0.0 copy-start.7
  10.0 0.9 %copy-done.7 = bf16[512,256]{1,0:T(8,128)(2,1)S(1)} copy-done((bf16[512,256]{1,0:T(8,128)(2,1)S(1)}, bf16[512,256]{1,0:T(8,128)(2,1)}, u32[]{:S(2)}) %copy-start.7) | copy-done | bytes 262168
  11.0 0.0 copy-start.8
  11.0 0.8 copy-done.8
  11.8 0.0 copy-start.9
  11.8 0.8 copy-done.9
  12.6 0.0 copy-start.10
  12.6 0.7 copy-done.10
  13.3 0.0 copy-start.11
  13.3 0.7 copy-done.11
  14.0 69.0 %fused_layer.1 = (bf16[16,512]{1,0:T(8,128)(2,1)S(1)}, f32[16,4,128,128]{3,2,1,0:T(8,128)}) custom-call(bf16[16,2048]{1,0:T(8,128)(2,1)S(1)} %copy-done.8, f32[16,4,128,128]{3,2,1,0:T(8,128)} %st_h.1, f32[1,512]{1,0:T(1,128)S(1)} %bitcast.2, f32[1,512]{1,0:T(1,128)S(1)} %bitcast.3, f32[4,2048]{1,0:T(4,128)S(1)} %copy-done.9, bf16[256,512]{1,0:T(8,128)(2,1)S(1)} %copy-done.3, ...), custom_call_target="tpu_custom_call" | custom-call | tf_op jit(solution)/shard_map/fused_layer/pallas_call | solution.py:702
  83.0 0.6 copy.25
  83.6 4.7 %copy.26 = f32[16,4,128,128]{3,2,1,0:T(8,128)} copy(f32[16,4,128,128]{3,2,1,0:T(8,128)} %get-tuple-element.5) | data formatting | bytes 8388608
Async XLA Ops:
  2.8 1.1 %copy-start = (bf16[256,1536]{1,0:T(8,128)(2,1)S(1)}, bf16[256,1536]{1,0:T(8,128)(2,1)}, u32[]{:S(2)}) copy-start(bf16[256,1536]{1,0:T(8,128)(2,1)} %dg_h.1) | copy-start | bytes 2359300
  4.0 1.1 %copy-start.1 = (bf16[256,1536]{1,0:T(8,128)(2,1)S(1)}, bf16[256,1536]{1,0:T(8,128)(2,1)}, u32[]{:S(2)}) copy-start(bf16[256,1536]{1,0:T(8,128)(2,1)} %du_h.1) | copy-start | bytes 2359300
  5.1 1.1 %copy-start.2 = (bf16[1536,256]{1,0:T(8,128)(2,1)S(1)}, bf16[1536,256]{1,0:T(8,128)(2,1)}, u32[]{:S(2)}) copy-start(bf16[1536,256]{1,0:T(8,128)(2,1)} %dd_h.1) | copy-start | bytes 2359300
  6.2 0.9 %copy-start.3 = (bf16[256,512]{1,0:T(8,128)(2,1)S(1)}, bf16[256,512]{1,0:T(8,128)(2,1)}, u32[]{:S(2)}) copy-start(bf16[256,512]{1,0:T(8,128)(2,1)} %wq_h.1) | copy-start | bytes 786436
  7.2 0.9 %copy-start.4 = (bf16[256,512]{1,0:T(8,128)(2,1)S(1)}, bf16[256,512]{1,0:T(8,128)(2,1)}, u32[]{:S(2)}) copy-start(bf16[256,512]{1,0:T(8,128)(2,1)} %wf_h.1) | copy-start | bytes 786436
  8.1 0.9 %copy-start.5 = (bf16[256,512]{1,0:T(8,128)(2,1)S(1)}, bf16[256,512]{1,0:T(8,128)(2,1)}, u32[]{:S(2)}) copy-start(bf16[256,512]{1,0:T(8,128)(2,1)} %wv_h.1) | copy-start | bytes 786436
  9.1 0.9 %copy-start.6 = (bf16[256,512]{1,0:T(8,128)(2,1)S(1)}, bf16[256,512]{1,0:T(8,128)(2,1)}, u32[]{:S(2)}) copy-start(bf16[256,512]{1,0:T(8,128)(2,1)} %wo_h.1) | copy-start | bytes 786436
  10.0 0.9 %copy-start.7 = (bf16[512,256]{1,0:T(8,128)(2,1)S(1)}, bf16[512,256]{1,0:T(8,128)(2,1)}, u32[]{:S(2)}) copy-start(bf16[512,256]{1,0:T(8,128)(2,1)} %wm_h.1) | copy-start | bytes 786436
  11.0 0.8 copy-start.8
  11.8 0.8 copy-start.9
  12.6 0.7 copy-start.10
  13.3 0.7 copy-start.11

commit v2 on v1

--- a/solution.py
+++ b/solution.py
@@ -197,7 +197,7 @@
     heads, hs = old_state.shape[1:3]
     block, part = width // n_ep, width // n_tp
     chans = heads * hs
-    topk = routes.shape[1]
+    topk = routes.shape[0]
     cap = max(2, 2 * seqs * topk // n_ep)
     cells, rows = n_ep * cap, n_ep * seqs
     eff, dff = experts[0].shape[2], dense[0].shape[1]
@@ -229,7 +229,7 @@
         tok_h, st_h, lb_h, hg_h, gn_h, wq_h, wf_h, wv_h, wo_h, wm_h, rt_h, sc_h,
         eg_h, eu_h, ed_h, dg_h, du_h, dd_h, mr_h,
         out, ns,
-        tok, st, lb, hg, gn, win, wm, rt0, sc, wgu, wed, wd, wdd, mrow,
+        tok, st, lb, hg, gn, win, wm, rt0, sc, wgu, wed, wd, wdd, mrow, wide_row,
         R, RT, X, Y, Z, PR, rd, MA, TX, TR, MV, STAT, SX, SR, COL, OWN, SEL, MO, MR,
         DX, DY, DZ, DR, DH, OX, ER, hid, RX, RR, RB, RG, dd, ddr, sq, sqr,
         send, recv, lsem,
@@ -348,10 +348,18 @@
                 )
             PR[h, q] = (X[h, c, q].astype(f32) + Y[h, q].astype(f32)).astype(bf16)
 
-        named = RT[...].reshape(rows, topk)
+        short = lax.broadcasted_iota(i32, (rows, seqs), 1)
+        turn = lax.broadcasted_iota(i32, (rows, seqs), 0)
+        diagonal = short == turn - (turn // seqs) * seqs
+        named = []
+        for k in range(topk):
+            across = jnp.concatenate(
+                [jnp.broadcast_to(RT[e, k : k + 1, :], (seqs, seqs)) for e in range(n_ep)], axis=0
+            )
+            named.append(jnp.sum(jnp.where(diagonal, across, 0), axis=1, keepdims=True))
         lane = lax.broadcasted_iota(i32, (rows, lanes), 1)
         row = lax.broadcasted_iota(i32, (rows, lanes), 0)
-        ones = [(lane == named[:, k : k + 1]).astype(f32) for k in range(topk)]
+        ones = [(lane == named[k]).astype(f32) for k in range(topk)]
         earlier = ((lane < row) & (lane >= (row // seqs) * seqs)).astype(bf16)
         before = dot32(earlier, sum(ones).astype(bf16))
         slots = [
@@ -361,19 +369,24 @@
         wide = lax.broadcasted_iota(i32, (rows, n_ep * cells), 1)
         chosen = jnp.zeros((rows, n_ep * cells), f32)
         for k in range(topk):
-            place = named[:, k : k + 1] * cells + spot * cap + slots[k]
+            place = named[k] * cells + spot * cap + slots[k]
             chosen = chosen + (wide == place).astype(f32)
         for i in range(n_ep * cells // lanes):
             SEL[i * lanes : (i + 1) * lanes, :] = chosen[:, i * lanes : (i + 1) * lanes].T.astype(bf16)
         ours = jnp.zeros((rows, lanes), i32)
         for k in range(topk):
-            ours = ours + jnp.where(lane == k, named[:, k : k + 1] * cap + slots[k], 0)
+            ours = ours + jnp.where(lane == k, named[k] * cap + slots[k], 0)
         OWN[...] = ours
         for copy in l_small:
             copy.wait()
+        wide_row[...] = mrow[...].astype(f32)
         at_own = OWN[own_rows, :]
         spread = lax.broadcasted_iota(i32, (seqs, cells), 1)
-        gap = sc[:, 0:1] - sc[:, 1:2]
+        gap = jnp.sum(
+            jnp.where(diagonal[0:seqs], jnp.broadcast_to(sc[0:1, :] - sc[1:2, :], (seqs, seqs)), 0.0),
+            axis=1,
+            keepdims=True,
+        )
         table = jnp.where(spread == at_own[:, 0:1], jax.nn.sigmoid(gap), 0.0)
         table = table + jnp.where(spread == at_own[:, 1:2], jax.nn.sigmoid(-gap), 0.0)
 
@@ -441,7 +454,13 @@
                     P_TP[1] + kk * n_tp + me_t,
                 )
         lane_duo = lax.broadcasted_iota(i32, (duo, lanes), 1)
-        mixer = mrow[0:1, mine].astype(f32)
+        mixer = jnp.concatenate(
+            [
+                wide_row[pl.ds(me_e * (block // lanes) + i, 1), :]
+                for i in range(block // lanes)
+            ],
+            axis=1,
+        )
         for kk in chips:
             for _, t in tp_peers:
                 arrive(TX.at[0], TR.at[0, 0], P_TP[1] + kk * n_tp + t)
@@ -715,15 +734,16 @@
             f(*norm_gains.shape),
             b(heads, block, 4 * hs),
             b(chans, block),
-            n(seqs, topk),
-            f(seqs, topk),
+            n(topk, seqs),
+            f(topk, seqs),
             b(width, 2 * eff),
             b(eff, width),
             b(CHUNKS, block, 2 * chunk),
             b(dff, block),
-            b(1, width),
+            b(width // lanes, lanes),
+            f(width // lanes, lanes),
             b(n_ep, seqs, block),
-            n(n_ep, seqs, topk),
+            n(n_ep, topk, seqs),
             b(heads, 2, half, seqs, 4 * hs),
             b(heads, half, seqs, 4 * hs),
             b(heads, half, seqs, 4 * hs),
@@ -762,22 +782,27 @@
             pltpu.SemaphoreType.DMA((n_load,)),
         ],
         compiler_params=pltpu.CompilerParams(
-            collective_id=1, has_side_effects=True, vmem_limit_bytes=48 * 1024 * 1024
+            collective_id=1, has_side_effects=True, vmem_limit_bytes=40 * 1024 * 1024
         ),
         name="fused_layer",
     )(
-        tokens,
-        old_state,
-        bounds,
-        head_gain,
-        norm_gains,
-        *in_weights,
-        w_mix,
-        routes,
-        scores,
-        *experts,
-        *dense,
-        mix_row,
+        *(
+            pltpu.with_memory_space_constraint(x, pltpu.HBM)
+            for x in (
+                tokens,
+                old_state,
+                bounds,
+                head_gain,
+                norm_gains,
+                *in_weights,
+                w_mix,
+                routes,
+                scores,
+                *experts,
+                *dense,
+                mix_row,
+            )
+        )
     )
 
 
@@ -810,11 +835,11 @@
         norm_gains,
         (w_query, w_forget, w_value, w_outgate),
         w_mix_out,
-        routes,
-        route_scores,
+        routes.T,
+        route_scores.T,
         (w_exp_gate, w_exp_up, w_exp_down),
         (w_dense_gate, w_dense_up, w_dense_down),
-        dense_mix[None, :],
+        dense_mix.reshape(-1, 128),
         lax.axis_size("ep"),
         lax.axis_size("tp"),
     )

time: 89 us -> 70.1 us (0.79)
  local copies, waits for them, and re-layouts: 18.6 us -> 2.62 us
  Pallas kernels: 69 us -> 66.7 us
    unnamed x28 -> x2, local copies, waits for them, and re-layouts: 17.9 us -> 2.62 us
    pallas_call x1, Pallas kernels: 69 us -> 66.7 us  [fused_layer(): pl.pallas_call(kernel, out_shape=(jax.ShapeDtypeStruct((seqs, part), bf16...]
where the time goes in v2:
time: 70.1 us; the launch traced here: 69.9 us
  Pallas kernels  66.7 us (95%)
  local copies, waits for them, and re-layouts  2.62 us (4%)
    pallas_call x1, Pallas kernels, fused_layer(): pl.pallas_call(kernel, out_shape=(jax.ShapeDtypeStruct((seqs, part), bf16...  66.7 us
    unnamed x2, local copies, waits for them, and re-layouts  2.62 us

profile of v2, /device:TPU:0, one launch (start us, length us, event | category | flops | bytes accessed | tf_op | source)
XLA Modules:
  0.0 69.9 jit_solution(17319231510867676267)
XLA Ops:
  0.6 66.7 %fused_layer.1 = (bf16[16,512]{1,0:T(8,128)(2,1)S(1)}, f32[16,4,128,128]{3,2,1,0:T(8,128)S(1)}) custom-call(bf16[16,2048]{1,0:T(8,128)(2,1)} %tok_h.1, f32[16,4,128,128]{3,2,1,0:T(8,128)} %st_h.1, f32[1,512]{1,0:T(1,128)} %bitcast.6, f32[1,512]{1,0:T(1,128)} %bitcast.7, f32[4,2048]{1,0:T(4,128)} %gn_h.1, bf16[256,512]{1,0:T(8,128)(2,1)} %wq_h.1, ...), custom_call_target="tpu_custom_call" | custom-call | tf_op jit(solution)/shard_map/fused_layer/pallas_call | solution.py:721
  67.3 0.6 copy.23
  67.9 2.0 %copy.24 = f32[16,4,128,128]{3,2,1,0:T(8,128)} copy(f32[16,4,128,128]{3,2,1,0:T(8,128)S(1)} %get-tuple-element.5) | data formatting | bytes 8388608

commit v3 on v2

--- a/solution.py
+++ b/solution.py
@@ -173,7 +173,7 @@
     return [q] + [lax.rem(q + k, half) for k in range(1, half)]
 
 
-CHUNKS = 2
+CHUNKS = 3
 
 
 def fused_layer(
@@ -206,32 +206,27 @@
     lanes = 128
     tile = 128
     chunk = dff // CHUNKS
+    hc = chunk // 2
 
     send_at, recv_at = Sems(), Sems()
 
     def pair(count):
-        return send_at.take(count), recv_at.take(count)
-
-    P_TOK, P_ROUTE = pair(n_ep), pair(n_ep)
-    P_PAIR, P_HEAD = pair(heads), pair(heads * half)
-    P_MIX = pair(heads * n_ep)
-    P_TP = pair(half * n_tp)
-    P_STAT, P_OWN = pair(n_ep), pair(n_ep)
-    P_DPAIR, P_DENSE = pair(CHUNKS), pair(CHUNKS * half)
-    P_EXP = pair(n_ep)
-    P_RTP, P_RET = pair(n_tp), pair(n_ep)
-    P_GATH, P_HAND = pair(CHUNKS * (half + 1)), pair(CHUNKS * (half + 1))
-    P_COLS = send_at.take(n_ep), recv_at.take(ratio * n_tp)
-    P_SQ = pair(n_tp)
-    n_load = 16 + 4 * heads + 2 * CHUNKS + 2 * (eff // tile)
+        return send_at.take(1), recv_at.take(count)
+
+    P_TOK, P_ROUTE, P_PAIR, P_HEAD = pair(1), pair(1), pair(heads), pair(heads)
+    P_MIX, P_TP, P_STAT, P_OWN = pair(half), pair(half), pair(1), pair(ratio)
+    P_SWAP, P_TWIN, P_DENSE = pair(CHUNKS), pair(2), pair(CHUNKS)
+    P_ROWS, P_EXP, P_RTP, P_RET = pair(1), pair(1), pair(1), pair(1)
+    P_GATH, P_HAND, P_COLS, P_SQ = pair(CHUNKS), pair(CHUNKS), pair(1), pair(1)
+    n_load = 13 + CHUNKS
 
     def kernel(
         tok_h, st_h, lb_h, hg_h, gn_h, wq_h, wf_h, wv_h, wo_h, wm_h, rt_h, sc_h,
         eg_h, eu_h, ed_h, dg_h, du_h, dd_h, mr_h,
         out, ns,
         tok, st, lb, hg, gn, win, wm, rt0, sc, wgu, wed, wd, wdd, mrow, wide_row,
-        R, RT, X, Y, Z, PR, rd, MA, TX, TR, MV, STAT, SX, SR, COL, OWN, SEL, MO, MR,
-        DX, DY, DZ, DR, DH, OX, ER, hid, RX, RR, RB, RG, dd, ddr, sq, sqr,
+        R, RP, RT, X, Y, Z, PR, rd, KC, VL, MA, TX, TR, STAT, SX, SR, COL, OWN, SEL, MO, MP, MR,
+        FF, DX, DR, DH, OT, OX, ET, ER, EI, hid, RX, RR, RB, RG, dd, ddr, sq, sqr,
         send, recv, lsem,
     ):
         me_e, me_t = lax.axis_index("ep"), lax.axis_index("tp")
@@ -250,56 +245,75 @@
 
         count = [0]
 
-        def load(src, dst):
-            copy = pltpu.make_async_copy(src, dst, lsem.at[count[0]])
+        def load(whole, *copies):
+            at = count[0]
             count[0] += 1
-            copy.start()
-            return copy
-
-        l_tok = load(tok_h, tok)
-        l_gn = load(gn_h, gn)
-        l_rt = load(rt_h, rt0)
-        l_in = [
-            [
-                load(w.at[:, h * hs : (h + 1) * hs], win.at[h, :, i * hs : (i + 1) * hs])
+            for src, dst in copies:
+                pltpu.make_async_copy(src, dst, lsem.at[at]).start()
+            return pltpu.make_async_copy(whole, whole, lsem.at[at])
+
+        l_tok = load(tok, (tok_h, tok))
+        l_gn = load(gn, (gn_h, gn))
+        l_rt = load(rt0, (rt_h, rt0))
+        l_in = load(
+            win,
+            *(
+                (w.at[:, h * hs : (h + 1) * hs], win.at[h, :, i * hs : (i + 1) * hs])
+                for h in range(heads)
                 for i, w in enumerate((wq_h, wf_h, wv_h, wo_h))
-            ]
-            for h in range(heads)
+            ),
+        )
+        l_small = [
+            load(v, (h, v)) for h, v in ((lb_h, lb), (hg_h, hg), (sc_h, sc), (mr_h, mrow))
         ]
-        l_small = [load(lb_h, lb), load(hg_h, hg), load(sc_h, sc), load(mr_h, mrow)]
-        l_st = load(st_h, st)
-        l_wm = load(wm_h, wm)
+        l_st = load(st, (st_h, st))
+        l_wm = load(wm, (wm_h, wm))
         l_wd = [
-            [
-                load(w.at[:, j * chunk : (j + 1) * chunk], wd.at[j, :, i * chunk : (i + 1) * chunk])
-                for i, w in enumerate((dg_h, du_h))
-            ]
+            load(
+                wd.at[j, 0],
+                *(
+                    (
+                        w.at[:, pl.ds(pl.multiple_of(j * chunk + c * hc, 128), hc)],
+                        wd.at[j, c, :, i * hc : (i + 1) * hc],
+                    )
+                    for i, w in enumerate((dg_h, du_h))
+                ),
+            )
             for j in range(CHUNKS)
         ]
-        l_exp = []
-        for i in range(eff // tile):
-            for k, w in enumerate((eg_h, eu_h)):
-                at = (2 * i + k) * tile
-                l_exp.append(load(w.at[0, :, i * tile : (i + 1) * tile], wgu.at[:, at : at + tile]))
-        l_exp.append(load(ed_h.at[0], wed))
-        l_wdd = load(dd_h, wdd)
-
-        sent = []
+        l_exp = [
+            load(
+                wgu,
+                *(
+                    (
+                        w.at[0, :, i * tile : (i + 1) * tile],
+                        wgu.at[:, (2 * i + k) * tile : (2 * i + k + 1) * tile],
+                    )
+                    for i in range(eff // tile)
+                    for k, w in enumerate((eg_h, eu_h))
+                ),
+            ),
+            load(wed, (ed_h.at[0], wed)),
+        ]
+        l_wdd = load(wdd, (dd_h, wdd))
 
         def put(src, dst, device, s, r):
-            copy = pltpu.make_async_remote_copy(
+            pltpu.make_async_remote_copy(
                 src_ref=src,
                 dst_ref=dst,
                 send_sem=send.at[s],
                 recv_sem=recv.at[r],
                 device_id=device,
                 device_id_type=MESH,
-            )
-            copy.start()
-            sent.append(copy.wait_send)
-
-        def arrive(like, dst, r):
-            pltpu.make_async_copy(like, dst, recv.at[r]).wait()
+            ).start()
+
+        def arrive(whole, r):
+            pltpu.make_async_copy(whole, whole, recv.at[r]).wait()
+
+        def left(whole, s):
+            pltpu.make_async_copy(whole, whole, send.at[s]).wait()
+
+        others, peers, far = n_ep - 1, n_tp - 1, half - 1
 
         def cut(first, size):
             return pl.ds(pl.multiple_of(first, 128), size)
@@ -312,9 +326,18 @@
         l_rt.wait()
         pl.semaphore_wait(barrier, n_ep + n_tp - 2)
         for de, e in ep_peers:
-            put(tok.at[:, cut(e * block, block)], R.at[me_e], (e, me_t), P_TOK[0] + de, P_TOK[1] + de)
+            put(tok.at[:, cut(e * block, block)], R.at[me_e], (e, me_t), P_TOK[0], P_TOK[1])
         for de, e in ep_peers:
-            put(rt0, RT.at[me_e], (e, me_t), P_ROUTE[0] + de, P_ROUTE[1] + de)
+            put(rt0, RT.at[me_e], (e, me_t), P_ROUTE[0], P_ROUTE[1])
+        for j in range(CHUNKS):
+            for i, w in enumerate((dg_h, du_h)):
+                put(
+                    w.at[:, cut(j * chunk + (1 - c) * hc, hc)],
+                    wd.at[j, c, :, i * hc : (i + 1) * hc],
+                    (partner, me_t),
+                    P_SWAP[0],
+                    P_SWAP[1] + j,
+                )
         R[me_e] = tok[:, mine]
         RT[me_e] = rt0[...]
         resid = tok[...].astype(f32)
@@ -322,32 +345,39 @@
         g0 = gn[0:1, mine]
         g1 = gn[1:2, mine]
         g2 = gn[2:3, mine]
-        for group in l_in:
-            for copy in group:
-                copy.wait()
-        for de, _ in ep_peers:
-            arrive(rt0, RT.at[0], P_ROUTE[1] + de)
-            arrive(tok.at[:, 0:block], R.at[0], P_TOK[1] + de)
+        l_in.wait()
+        arrive(R.at[0:others], P_TOK[1])
 
         scaled = (R[...].reshape(rows, block).astype(f32) * g0).astype(bf16)
-        for h in range(heads):
+
+        def project(h):
             piece = dot32(scaled, win[h]).astype(bf16)
             for e in range(n_ep):
                 X[h, e % 2, e // 2] = piece[e * seqs : (e + 1) * seqs]
-            put(X.at[h, 1 - c], Y.at[h], (partner, me_t), P_PAIR[0] + h, P_PAIR[1] + h)
-        for h in range(heads):
-            arrive(X.at[h, 0], Y.at[h], P_PAIR[1] + h)
-            for k, kk in enumerate(away):
+            put(X.at[h, 1 - c], Y.at[h], (partner, me_t), P_PAIR[0], P_PAIR[1] + h)
+
+        def spread_head(h):
+            arrive(Y.at[h], P_PAIR[1] + h)
+            for kk in away:
                 Z[h, kk] = (X[h, c, kk].astype(f32) + Y[h, kk].astype(f32)).astype(bf16)
                 put(
                     Z.at[h, kk],
                     PR.at[h, q],
                     (2 * kk + c, me_t),
-                    P_HEAD[0] + h * half + k,
-                    P_HEAD[1] + h * half + q,
+                    P_HEAD[0],
+                    P_HEAD[1] + h,
                 )
             PR[h, q] = (X[h, c, q].astype(f32) + Y[h, q].astype(f32)).astype(bf16)
 
+        project(0)
+        project(1)
+        for h in range(heads):
+            spread_head(h)
+            if h + 2 < heads:
+                project(h + 2)
+        put(R, RP, (partner, me_t), P_TWIN[0], P_TWIN[1])
+
+        arrive(RT.at[0:others], P_ROUTE[1])
         short = lax.broadcasted_iota(i32, (rows, seqs), 1)
         turn = lax.broadcasted_iota(i32, (rows, seqs), 0)
         diagonal = short == turn - (turn // seqs) * seqs
@@ -373,6 +403,10 @@
             chosen = chosen + (wide == place).astype(f32)
         for i in range(n_ep * cells // lanes):
             SEL[i * lanes : (i + 1) * lanes, :] = chosen[:, i * lanes : (i + 1) * lanes].T.astype(bf16)
+        picked = dot32(SEL[...], R[...].reshape(rows, block)).astype(bf16)
+        for e in range(n_ep):
+            OT[e] = picked[e * cells : (e + 1) * cells]
+        ET[:, mine] = OT[me_e]
         ours = jnp.zeros((rows, lanes), i32)
         for k in range(topk):
             ours = ours + jnp.where(lane == k, named[k] * cap + slots[k], 0)
@@ -392,8 +426,7 @@
 
         l_st.wait()
         for h in range(heads):
-            for kk in chips[1:]:
-                arrive(Z.at[h, 0], PR.at[h, 0], P_HEAD[1] + h * half + kk)
+            arrive(PR.at[h, 0:far], P_HEAD[1] + h)
             total = PR[h, 0].astype(f32)
             for kk in range(1, half):
                 total = total + PR[h, kk].astype(f32)
@@ -406,18 +439,15 @@
             query = silu(total[:, 0:hs])
             value = total[:, 2 * hs : 3 * hs]
             columns = jnp.concatenate(
-                [forget, key_in, query, jnp.zeros((hs - 3 * seqs, hs), f32)], axis=0
+                [forget, key_in, query * forget, jnp.zeros((hs - 3 * seqs, hs), f32)], axis=0
             ).T
+            KC[h] = columns
+            VL[h] = value
             for s in range(seqs):
-                new = (
-                    columns[:, s : s + 1] * st[s, h]
-                    + columns[:, seqs + s : seqs + s + 1] * value[s : s + 1, :]
+                rd[s : s + 1, :] = jnp.sum(
+                    columns[:, 2 * seqs + s : 2 * seqs + s + 1] * st[s, h], axis=0, keepdims=True
                 )
-                ns[s, h] = new
-                rd[s : s + 1, :] = jnp.sum(
-                    columns[:, 2 * seqs + s : 2 * seqs + s + 1] * new, axis=0, keepdims=True
-                )
-            read = rd[...]
+            read = rd[...] + jnp.sum(query * key_in, axis=1, keepdims=True) * value
             gated = read * rms_scale(read) * hg[0:1, at] * silu(total[:, 3 * hs :])
             MA[h, me_e] = gated.astype(bf16)
             for de, e in ep_peers:
@@ -425,20 +455,26 @@
                     MA.at[h, me_e],
                     MA.at[h, me_e],
                     (e, me_t),
-                    P_MIX[0] + h * n_ep + de,
-                    P_MIX[1] + h * n_ep + me_e,
+                    P_MIX[0],
+                    P_MIX[1] + q,
                 )
+
+        for de, e in ep_peers:
+            put(OT.at[e], ET.at[:, mine], (e, me_t), P_ROWS[0], P_ROWS[1])
+
+        def update(h):
+            for s in range(seqs):
+                ns[s, h] = (
+                    KC[h, :, s : s + 1] * st[s, h]
+                    + KC[h, :, seqs + s : seqs + s + 1] * VL[h, s : s + 1, :]
+                )
+
+        update(0)
+        update(1)
 
         l_wm.wait()
         for g, kk in enumerate(chips):
-            for e in (2 * kk, 2 * kk + 1):
-                if g == 0:
-                    continue
-                for h in range(heads):
-                    arrive(MA.at[h, 0], MA.at[h, 1], P_MIX[1] + h * n_ep + e)
-            if g == 0:
-                for h in range(heads):
-                    arrive(MA.at[h, 0], MA.at[h, 1], P_MIX[1] + h * n_ep + partner)
+            arrive(MA.at[:, 0 : 2 if g else 1], P_MIX[1] + kk)
             lhs = jnp.concatenate(
                 [MA[h, pl.ds(2 * kk, 2)].reshape(duo, hs) for h in range(heads)], axis=1
             )
@@ -450,8 +486,8 @@
                     TX.at[kk],
                     TR.at[me_t, kk],
                     (me_e, t),
-                    P_TP[0] + g * n_tp + dt,
-                    P_TP[1] + kk * n_tp + me_t,
+                    P_TP[0],
+                    P_TP[1] + kk,
                 )
         lane_duo = lax.broadcasted_iota(i32, (duo, lanes), 1)
         mixer = jnp.concatenate(
@@ -462,15 +498,13 @@
             axis=1,
         )
         for kk in chips:
-            for _, t in tp_peers:
-                arrive(TX.at[0], TR.at[0, 0], P_TP[1] + kk * n_tp + t)
+            arrive(TR.at[0:peers, 0], P_TP[1] + kk)
             total = TR[0, kk].astype(f32)
             for t in range(1, n_tp):
                 total = total + TR[t, kk].astype(f32)
             narrow = total.astype(bf16)
             MO[pl.ds(2 * kk, 2)] = narrow.reshape(2, seqs, block)
             mixed = narrow.astype(f32)
-            MV[kk] = mixed
             base = R[pl.ds(2 * kk, 2)].reshape(duo, block).astype(f32)
             lifted = mixed * g1
             figures = (
@@ -490,36 +524,34 @@
         SX[...] = STAT[...].reshape(rows, lanes).T[0:8, :]
         SR[me_e] = SX[...]
         for de, e in ep_peers:
-            put(SX, SR.at[me_e], (e, me_t), P_STAT[0] + de, P_STAT[1] + de)
+            put(SX, SR.at[me_e], (e, me_t), P_STAT[0], P_STAT[1])
+        put(MO, MP, (partner, me_t), P_TWIN[0], P_TWIN[1] + 1)
+        picked = dot32(SEL[...], MO[...].reshape(rows, block)).astype(bf16)
+        for e in range(n_ep):
+            OX[e] = picked[e * cells : (e + 1) * cells]
+        for de, e in ep_peers:
+            put(OX.at[e], ER.at[:, mine], (e, me_t), P_EXP[0], P_EXP[1])
+        ER[:, mine] = OX[me_e]
 
         def send_own():
-            for de, e in ep_peers:
-                pltpu.make_async_remote_copy(
-                    src_ref=MO.at[e],
-                    dst_ref=MR.at[lax.rem(me_e, ratio)],
-                    send_sem=send.at[P_OWN[0] + de],
-                    recv_sem=recv.at[P_OWN[1] + lax.rem(me_e, ratio)],
-                    device_id=(e, me_t),
-                    device_id_type=MESH,
-                ).start()
+            for _, e in ep_peers:
+                put(
+                    MO.at[e],
+                    MR.at[lax.rem(me_e, ratio)],
+                    (e, me_t),
+                    P_OWN[0],
+                    P_OWN[1] + lax.rem(me_e, ratio),
+                )
             MR[lax.rem(me_e, ratio)] = MO[me_e]
-
-        def sent_own():
-            for de, e in ep_peers:
-                pltpu.make_async_remote_copy(
-                    src_ref=MO.at[e],
-                    dst_ref=MR.at[lax.rem(me_e, ratio)],
-                    send_sem=send.at[P_OWN[0] + de],
-                    recv_sem=recv.at[P_OWN[1] + lax.rem(me_e, ratio)],
-                    device_id=(e, me_t),
-                    device_id_type=MESH,
-                ).wait_send()
 
         holds = me_e // ratio == me_t
         pl.when(holds)(send_own)
-
-        for de, _ in ep_peers:
-            arrive(SX, SR.at[0], P_STAT[1] + de)
+        update(2)
+        update(3)
+        arrive(RP, P_TWIN[1])
+        arrive(MP, P_TWIN[1] + 1)
+
+        arrive(SR.at[0:others], P_STAT[1])
         total = SR[0]
         for e in range(1, n_ep):
             total = total + SR[e]
@@ -530,100 +562,86 @@
         back = jnp.where(row == 0, inv_mix, jnp.where(row == 1, inv_after, jnp.where(row == 2, weight, 0.0)))
         back = back.T
         COL[...] = back
-        after = R[...].reshape(rows, block).astype(f32) + MV[...].reshape(rows, block) * back[:, 0:1] * g1
-        ffn_in = (after * back[:, 1:2] * g2).astype(bf16)
-
-        step = 256
+        def normed(base, mixed, device):
+            at = cut(device * block, block)
+            after = base[...].reshape(rows, block).astype(f32)
+            after = after + mixed[...].reshape(rows, block).astype(f32) * back[:, 0:1] * gn[1:2, at]
+            return (after * back[:, 1:2] * gn[2:3, at]).astype(bf16)
+
+        FF[c] = normed(R, MO, me_e)
+        FF[1 - c] = normed(RP, MP, partner)
+
         for j in range(CHUNKS):
-            for copy in l_wd[j]:
-                copy.wait()
-            for a in range(0, 2 * chunk, step):
-                piece = dot32(ffn_in, wd[j, :, a : a + step]).astype(bf16)
-                for e in range(n_ep):
-                    DX[j, e % 2, e // 2, :, a : a + step] = piece[e * seqs : (e + 1) * seqs]
-            put(DX.at[j, 1 - c], DY.at[j], (partner, me_t), P_DPAIR[0] + j, P_DPAIR[1] + j)
-            if j == 0:
-                routed = dot32(SEL[...], ffn_in).astype(bf16)
-                for e in range(n_ep):
-                    OX[e] = routed[e * cells : (e + 1) * cells]
-                for de, e in ep_peers:
-                    put(OX.at[e], ER.at[:, mine], (e, me_t), P_EXP[0] + de, P_EXP[1] + de)
-                ER[:, mine] = OX[me_e]
-        for j in range(CHUNKS):
-            arrive(DX.at[j, 0], DY.at[j], P_DPAIR[1] + j)
-            for k, kk in enumerate(away):
-                DZ[j, kk] = (DX[j, c, kk].astype(f32) + DY[j, kk].astype(f32)).astype(bf16)
+            l_wd[j].wait()
+            arrive(wd.at[j, 0], P_SWAP[1] + j)
+            piece = (dot32(FF[0], wd[j, 0]) + dot32(FF[1], wd[j, 1])).astype(bf16)
+            for kk in range(half):
+                DX[j, kk] = piece[kk * duo : (kk + 1) * duo]
+            for kk in away:
                 put(
-                    DZ.at[j, kk],
+                    DX.at[j, kk],
                     DR.at[j, q],
                     (2 * kk + c, me_t),
-                    P_DENSE[0] + j * half + k,
-                    P_DENSE[1] + j * half + q,
+                    P_DENSE[0],
+                    P_DENSE[1] + j,
                 )
-            DR[j, q] = (DX[j, c, q].astype(f32) + DY[j, q].astype(f32)).astype(bf16)
+            DR[j, q] = DX[j, q]
+
+        def hidden(j):
+            arrive(DR.at[j, 0:far], P_DENSE[1] + j)
+            total = DR[j, 0].astype(f32)
+            for kk in range(1, half):
+                total = total + DR[j, kk].astype(f32)
+            here = DH.at[j, c, q]
+            here[...] = (silu(total[:, :hc]) * total[:, hc:]).astype(bf16)
+            for kk in away:
+                put(here, here, (2 * kk + c, me_t), P_GATH[0], P_GATH[1] + j)
+            put(here, here, (partner, me_t), P_HAND[0], P_HAND[1] + j)
+
+        def hand_over(j):
+            arrive(DH.at[j, 0, 0:far], P_GATH[1] + j)
+            for kk in away:
+                here = DH.at[j, c, kk]
+                put(here, here, (partner, me_t), P_HAND[0], P_HAND[1] + j)
+
+        def gathered(j):
+            arrive(DH.at[j, 0], P_HAND[1] + j)
+            total = 0.0
+            for i in range(2):
+                at = j * chunk + i * hc
+                total = total + dot32(DH[j, i].reshape(rows, hc), wdd[at : at + hc, :])
+            return total
 
         for copy in l_exp:
             copy.wait()
-        for de, _ in ep_peers:
-            arrive(OX.at[0], ER.at[:, 0:block], P_EXP[1] + de)
+        arrive(OT.at[0:others], P_ROWS[1])
+        arrive(OX.at[0:others], P_EXP[1])
+        marks = jnp.dot(
+            SEL[pl.ds(pl.multiple_of(me_e * cells, cells), cells), :].astype(f32),
+            back,
+            precision=lax.Precision.HIGHEST,
+            preferred_element_type=f32,
+        )
+        for a in range(0, width, block):
+            at = slice(a, a + block)
+            after = ET[:, at].astype(f32) + ER[:, at].astype(f32) * marks[:, 0:1] * gn[1:2, at]
+            EI[:, at] = (after * marks[:, 1:2] * gn[2:3, at]).astype(bf16)
 
         @pl.loop(0, eff // tile)
         def _(i):
-            both = dot32(ER[...], wgu[:, cut(i * 2 * tile, 2 * tile)])
+            both = dot32(EI[...], wgu[:, cut(i * 2 * tile, 2 * tile)])
             hid[:, cut(i * tile, tile)] = (silu(both[:, :tile]) * both[:, tile:]).astype(bf16)
 
         for dt, t in tp_peers + [(0, me_t)]:
             piece = dot32(hid[...], wed[:, cut(t * part, part)]).astype(bf16)
             if dt:
                 RX[dt] = piece
-                put(RX.at[dt], RR.at[me_t], (me_e, t), P_RTP[0] + dt, P_RTP[1] + dt)
+                put(RX.at[dt], RR.at[me_t], (me_e, t), P_RTP[0], P_RTP[1])
             else:
                 RR[me_t] = piece
 
-        def hidden(j):
-            for kk in chips[1:]:
-                arrive(DZ.at[j, 0], DR.at[j, 0], P_DENSE[1] + j * half + kk)
-            for a in range(0, chunk, step):
-                gate = DR[j, 0, :, a : a + step].astype(f32)
-                up = DR[j, 0, :, chunk + a : chunk + a + step].astype(f32)
-                for kk in range(1, half):
-                    gate = gate + DR[j, kk, :, a : a + step].astype(f32)
-                    up = up + DR[j, kk, :, chunk + a : chunk + a + step].astype(f32)
-                DH[j, me_e, :, a : a + step] = (silu(gate) * up).astype(bf16)
-            base = j * (half + 1)
-            for k, kk in enumerate(away):
-                put(
-                    DH.at[j, me_e],
-                    DH.at[j, me_e],
-                    (2 * kk + c, me_t),
-                    P_GATH[0] + base + k,
-                    P_GATH[1] + base + q,
-                )
-            put(
-                DH.at[j, me_e],
-                DH.at[j, me_e],
-                (partner, me_t),
-                P_GATH[0] + base + half,
-                P_GATH[1] + base + half,
-            )
-
-        def hand_over(j):
-            base = j * (half + 1)
-            for k, kk in enumerate(chips[1:]):
-                arrive(DH.at[j, 0], DH.at[j, 1], P_GATH[1] + base + kk)
-                here = DH.at[j, 2 * kk + c]
-                put(here, here, (partner, me_t), P_HAND[0] + base + k, P_HAND[1] + base + kk)
-
-        def gathered(j):
-            base = j * (half + 1)
-            arrive(DH.at[j, 0], DH.at[j, 1], P_GATH[1] + base + half)
-            for kk in chips[1:]:
-                arrive(DH.at[j, 0], DH.at[j, 1], P_HAND[1] + base + kk)
-            return dot32(DH[j].reshape(rows, chunk), wdd[j * chunk : (j + 1) * chunk, :])
-
         def give_back():
-            for dt, _ in tp_peers:
-                arrive(RX.at[0], RR.at[0], P_RTP[1] + dt)
+            arrive(RR.at[0:peers], P_RTP[1])
             total = RR[0].astype(f32)
             for t in range(1, n_tp):
                 total = total + RR[t].astype(f32)
@@ -632,12 +650,11 @@
                 RB[e] = total[e * cap : (e + 1) * cap]
             RG[me_e] = RB[me_e]
             for de, e in ep_peers:
-                put(RB.at[e], RG.at[me_e], (e, me_t), P_RET[0] + de, P_RET[1] + de)
-
-        hidden(0)
+                put(RB.at[e], RG.at[me_e], (e, me_t), P_RET[0], P_RET[1])
+
+        for j in range(CHUNKS):
+            hidden(j)
         give_back()
-        for j in range(1, CHUNKS):
-            hidden(j)
         for j in range(CHUNKS):
             hand_over(j)
         l_wdd.wait()
@@ -648,29 +665,19 @@
         for e in range(n_ep):
             dd[e] = total[e * seqs : (e + 1) * seqs]
         to = me_e // ratio
-        slot = lax.rem(me_e, ratio) * n_tp + me_t
         landing = ddr.at[lax.rem(me_e, ratio), me_t]
-        for de in range(n_ep):
-            e = lax.rem(me_e + de, n_ep)
-            remote = pltpu.make_async_remote_copy(
-                src_ref=dd.at[e],
-                dst_ref=landing,
-                send_sem=send.at[P_COLS[0] + de],
-                recv_sem=recv.at[P_COLS[1] + slot],
-                device_id=(e, to),
-                device_id_type=MESH,
-            )
-            if de == 0:
-                own = pltpu.make_async_copy(dd.at[e], landing, recv.at[P_COLS[1] + slot])
-                pl.when(to == me_t)(own.start)
-                pl.when(to != me_t)(remote.start)
-                sent.append(lambda remote=remote: pl.when(to != me_t)(remote.wait_send))
-            else:
-                remote.start()
-                sent.append(remote.wait_send)
-
-        for de, _ in ep_peers:
-            arrive(RB.at[0], RG.at[0], P_RET[1] + de)
+        for _, e in ep_peers:
+            put(dd.at[e], landing, (e, to), P_COLS[0], P_COLS[1])
+
+        def keep():
+            landing[...] = dd[me_e]
+
+        pl.when(holds)(keep)
+        pl.when(jnp.logical_not(holds))(
+            lambda: put(dd.at[me_e], landing, (me_e, to), P_COLS[0], P_COLS[1])
+        )
+
+        arrive(RG.at[0:others], P_RET[1])
         expert_sum = jnp.dot(
             table,
             RG[...].astype(f32).reshape(cells, part),
@@ -683,13 +690,13 @@
             source = me_t * ratio + j
 
             def wait_own(j=j):
-                arrive(MO.at[0], MR.at[j], P_OWN[1] + j)
+                arrive(MR.at[j], P_OWN[1] + j)
 
             pl.when(source != me_e)(wait_own)
         mix_own = jnp.concatenate([MR[j].astype(f32) for j in range(ratio)], axis=1)
         after_own = tok[:, part_at].astype(f32) + mix_own * own_cols[:, 0:1] * gn[1:2, part_at]
-        for i in range(ratio * n_tp):
-            arrive(dd.at[0], ddr.at[i // n_tp, i % n_tp], P_COLS[1] + i)
+        pl.when(holds)(lambda: arrive(dd.at[0:others], P_COLS[1]))
+        pl.when(jnp.logical_not(holds))(lambda: arrive(dd, P_COLS[1]))
         pieces = []
         for j in range(ratio):
             total = ddr[j, 0].astype(f32)
@@ -701,17 +708,36 @@
         sq[...] = jnp.broadcast_to(mass, (seqs, lanes))
         sqr[me_t] = sq[...]
         for dt, t in tp_peers:
-            put(sq, sqr.at[me_t], (me_e, t), P_SQ[0] + dt, P_SQ[1] + dt)
-        for dt, _ in tp_peers:
-            arrive(sq, sqr.at[0], P_SQ[1] + dt)
+            put(sq, sqr.at[me_t], (me_e, t), P_SQ[0], P_SQ[1])
+        arrive(sqr.at[0:peers], P_SQ[1])
         total = sqr[0]
         for t in range(1, n_tp):
             total = total + sqr[t]
         scale = lax.rsqrt(total[:, 0:1] / width + EPS)
         out[...] = (after_own + ffn_out * scale * gn[3:4, part_at]).astype(bf16)
-        pl.when(holds)(sent_own)
-        for wait in sent:
-            wait()
+        pl.when(holds)(lambda: left(MO.at[0:others], P_OWN[0]))
+        pl.when(holds)(lambda: left(dd.at[0:others], P_COLS[0]))
+        pl.when(jnp.logical_not(holds))(lambda: left(dd, P_COLS[0]))
+        for whole, ends in (
+            (R.at[0:others], P_TOK),
+            (RT.at[0:others], P_ROUTE),
+            (Y, P_PAIR),
+            (Z.at[:, 0:far], P_HEAD),
+            (MA.at[:, 0:others], P_MIX),
+            (TR.at[0:peers], P_TP),
+            (SR.at[0:others], P_STAT),
+            (wd.at[:, 0], P_SWAP),
+            (FF, P_TWIN),
+            (OT.at[0:others], P_ROWS),
+            (OX.at[0:others], P_EXP),
+            (DX.at[:, 0:far], P_DENSE),
+            (DH.at[:, 0, 0:far], P_GATH),
+            (DH.at[:, 0], P_HAND),
+            (RR.at[0:peers], P_RTP),
+            (RB.at[0:others], P_RET),
+            (sqr.at[0:peers], P_SQ),
+        ):
+            left(whole, ends[0])
 
     vmem = pl.BlockSpec(memory_space=pltpu.VMEM)
     hbm = pl.BlockSpec(memory_space=pltpu.HBM)
@@ -722,7 +748,7 @@
         kernel,
         out_shape=(
             jax.ShapeDtypeStruct((seqs, part), bf16),
-            jax.ShapeDtypeStruct(old_state.shape, f32),
+            pltpu.VMEM(old_state.shape, f32),
         ),
         in_specs=[hbm] * 19,
         out_specs=(vmem, vmem),
@@ -738,10 +764,11 @@
             f(topk, seqs),
             b(width, 2 * eff),
             b(eff, width),
-            b(CHUNKS, block, 2 * chunk),
+            b(CHUNKS, 2, block, chunk),
             b(dff, block),
             b(width // lanes, lanes),
             f(width // lanes, lanes),
+            b(n_ep, seqs, block),
             b(n_ep, seqs, block),
             n(n_ep, topk, seqs),
             b(heads, 2, half, seqs, 4 * hs),
@@ -749,10 +776,11 @@
             b(heads, half, seqs, 4 * hs),
             b(heads, half, seqs, 4 * hs),
             f(seqs, hs),
+            f(heads, hs, hs),
+            f(heads, seqs, hs),
             b(heads, n_ep, seqs, hs),
             b(half, duo, block),
             b(n_tp, half, duo, block),
-            f(half, duo, block),
             f(half, duo, lanes),
             f(8, lanes),
             f(n_ep, 8, lanes),
@@ -760,13 +788,16 @@
             n(rows, lanes),
             b(n_ep * cells, rows),
             b(n_ep, seqs, block),
+            b(n_ep, seqs, block),
             b(ratio, seqs, block),
-            b(CHUNKS, 2, half, seqs, 2 * chunk),
-            b(CHUNKS, half, seqs, 2 * chunk),
-            b(CHUNKS, half, seqs, 2 * chunk),
-            b(CHUNKS, half, seqs, 2 * chunk),
-            b(CHUNKS, n_ep, seqs, chunk),
+            b(2, rows, block),
+            b(CHUNKS, half, duo, chunk),
+            b(CHUNKS, half, duo, chunk),
+            b(CHUNKS, 2, half, duo, hc),
             b(n_ep, cells, block),
+            b(n_ep, cells, block),
+            b(cells, width),
+            b(cells, width),
             b(cells, width),
             b(cells, eff),
             b(n_tp, cells, part),
@@ -806,6 +837,41 @@
     )
 
 
+PIECES = 16
+
+
+def write_out(layer_out, new_state):
+    per = new_state.shape[0] // PIECES
+
+    def kernel(small, big, small_to, big_to, sems):
+        copies = [pltpu.make_async_copy(small, small_to, sems.at[PIECES])]
+        for i in range(PIECES):
+            at = pl.ds(i * per, per)
+            copies.append(pltpu.make_async_copy(big.at[at], big_to.at[at], sems.at[i]))
+        for copy in copies:
+            copy.start()
+        for copy in copies:
+            copy.wait()
+
+    vmem = pl.BlockSpec(memory_space=pltpu.VMEM)
+    hbm = pl.BlockSpec(memory_space=pltpu.HBM)
+    return pl.pallas_call(
+        kernel,
+        out_shape=(
+            pltpu.HBM(layer_out.shape, layer_out.dtype),
+            pltpu.HBM(new_state.shape, new_state.dtype),
+        ),
+        in_specs=[vmem] * 2,
+        out_specs=(hbm, hbm),
+        scratch_shapes=[pltpu.SemaphoreType.DMA((PIECES + 1,))],
+        compiler_params=pltpu.CompilerParams(vmem_limit_bytes=1024 * 1024),
+        name="write_out",
+    )(
+        pltpu.with_memory_space_constraint(layer_out, pltpu.VMEM),
+        pltpu.with_memory_space_constraint(new_state, pltpu.VMEM),
+    )
+
+
 def fast_body(
     tokens,
     old_state,
@@ -827,7 +893,7 @@
     w_dense_down,
     dense_mix,
 ):
-    return fused_layer(
+    layer_out, new_state = fused_layer(
         tokens,
         old_state,
         lower_bound[None, :],
@@ -843,6 +909,7 @@
         lax.axis_size("ep"),
         lax.axis_size("tp"),
     )
+    return write_out(layer_out, new_state)
 
 
 def solution(mesh):

time: 70.1 us -> 63.6 us (0.907)
  Pallas kernels: 66.7 us -> 62.8 us
  local copies, waits for them, and re-layouts: 2.62 us -> 0 us
    pallas_call x1, Pallas kernels: 66.7 us -> 60.7 us  [fused_layer(): pl.pallas_call(kernel, out_shape=(jax.ShapeDtypeStruct((seqs, part), bf16...]
    unnamed x2 -> x0, local copies, waits for them, and re-layouts: 2.62 us -> none
    pallas_call x0 -> x1, Pallas kernels: none -> 2.15 us  [write_out(): pl.pallas_call(kernel, out_shape=(pltpu.HBM(layer_out.shape, layer_out.dt...]
where the time goes in v3:
time: 63.6 us; the launch traced here: 63.5 us
  Pallas kernels  62.8 us (99%)
  between operations  0.65 us (1%)
    pallas_call x1, Pallas kernels, fused_layer(): pl.pallas_call(kernel, out_shape=(jax.ShapeDtypeStruct((seqs, part), bf16...  60.7 us
    pallas_call x1, Pallas kernels, write_out(): pl.pallas_call(kernel, out_shape=(pltpu.HBM(layer_out.shape, layer_out.dt...  2.15 us

profile of v3, /device:TPU:0, one launch (start us, length us, event | category | flops | bytes accessed | tf_op | source)
XLA Modules:
  0.0 63.5 jit_solution(4344772100620163629)
XLA Ops:
  0.6 60.7 %fused_layer.1 = (bf16[16,512]{1,0:T(8,128)(2,1)S(1)}, f32[16,4,128,128]{3,2,1,0:T(8,128)S(1)}) custom-call(bf16[16,2048]{1,0:T(8,128)(2,1)} %tok_h.1, f32[16,4,128,128]{3,2,1,0:T(8,128)} %st_h.1, f32[1,512]{1,0:T(1,128)} %bitcast.6, f32[1,512]{1,0:T(1,128)} %bitcast.7, f32[4,2048]{1,0:T(4,128)} %gn_h.1, bf16[256,512]{1,0:T(8,128)(2,1)} %wq_h.1, ...), custom_call_target="tpu_custom_call" | custom-call | tf_op jit(solution)/shard_map/fused_layer/pallas_call | solution.py:747
  61.3 2.1 %write_out.1 = (bf16[16,512]{1,0:T(8,128)(2,1)}, f32[16,4,128,128]{3,2,1,0:T(8,128)}) custom-call(bf16[16,512]{1,0:T(8,128)(2,1)S(1)} %get-tuple-element.4.small, f32[16,4,128,128]{3,2,1,0:T(8,128)S(1)} %get-tuple-element.5.big), custom_call_target="tpu_custom_call" | custom-call | tf_op jit(solution)/shard_map/write_out/pallas_call | solution.py:858

commit v4 on v3

--- a/solution.py
+++ b/solution.py
@@ -207,6 +207,7 @@
     tile = 128
     chunk = dff // CHUNKS
     hc = chunk // 2
+    few = ratio * cap
 
     send_at, recv_at = Sems(), Sems()
 
@@ -215,8 +216,9 @@
 
     P_TOK, P_ROUTE, P_PAIR, P_HEAD = pair(1), pair(1), pair(heads), pair(heads)
     P_MIX, P_TP, P_STAT, P_OWN = pair(half), pair(half), pair(1), pair(ratio)
-    P_SWAP, P_TWIN, P_DENSE = pair(CHUNKS), pair(2), pair(CHUNKS)
-    P_ROWS, P_EXP, P_RTP, P_RET = pair(1), pair(1), pair(1), pair(1)
+    P_SWAP, P_TWIN, P_BASE, P_DENSE = pair(CHUNKS), pair(2), pair(1), pair(CHUNKS)
+    P_ROWS, P_EXP, P_ALL = pair(1), pair(1), pair(1)
+    P_RTP, P_RET = pair(1), pair(1)
     P_GATH, P_HAND, P_COLS, P_SQ = pair(CHUNKS), pair(CHUNKS), pair(1), pair(1)
     n_load = 13 + CHUNKS
 
@@ -226,7 +228,7 @@
         out, ns,
         tok, st, lb, hg, gn, win, wm, rt0, sc, wgu, wed, wd, wdd, mrow, wide_row,
         R, RP, RT, X, Y, Z, PR, rd, KC, VL, MA, TX, TR, STAT, SX, SR, COL, OWN, SEL, MO, MP, MR,
-        FF, DX, DR, DH, OT, OX, ET, ER, EI, hid, RX, RR, RB, RG, dd, ddr, sq, sqr,
+        FF, AX, AR, DX, DR, DH, OT, OX, ET, ER, EI, hid, RX, RR, RB, RG, dd, ddr, sq, sqr,
         send, recv, lsem,
     ):
         me_e, me_t = lax.axis_index("ep"), lax.axis_index("tp")
@@ -348,6 +350,7 @@
         l_in.wait()
         arrive(R.at[0:others], P_TOK[1])
 
+        put(R, RP, (partner, me_t), P_TWIN[0], P_TWIN[1])
         scaled = (R[...].reshape(rows, block).astype(f32) * g0).astype(bf16)
 
         def project(h):
@@ -375,7 +378,6 @@
             spread_head(h)
             if h + 2 < heads:
                 project(h + 2)
-        put(R, RP, (partner, me_t), P_TWIN[0], P_TWIN[1])
 
         arrive(RT.at[0:others], P_ROUTE[1])
         short = lax.broadcasted_iota(i32, (rows, seqs), 1)
@@ -401,11 +403,18 @@
         for k in range(topk):
             place = named[k] * cells + spot * cap + slots[k]
             chosen = chosen + (wide == place).astype(f32)
-        for i in range(n_ep * cells // lanes):
-            SEL[i * lanes : (i + 1) * lanes, :] = chosen[:, i * lanes : (i + 1) * lanes].T.astype(bf16)
-        picked = dot32(SEL[...], R[...].reshape(rows, block)).astype(bf16)
-        for e in range(n_ep):
-            OT[e] = picked[e * cells : (e + 1) * cells]
+        per = lanes // cells
+        for i in range(n_ep // per):
+            flipped = chosen[:, i * lanes : (i + 1) * lanes].T.astype(bf16)
+            SEL[i * per : (i + 1) * per] = flipped.reshape(per, n_tp, few, rows)
+
+        def pick(base, ox):
+            lhs = SEL[:, pl.ds(me_t, 1)].reshape(n_ep * few, rows)
+            picked = dot32(lhs, base[...].reshape(rows, block)).astype(bf16)
+            for e in range(n_ep):
+                ox[e] = picked[e * few : (e + 1) * few]
+
+        pick(R, OT)
         ET[:, mine] = OT[me_e]
         ours = jnp.zeros((rows, lanes), i32)
         for k in range(topk):
@@ -423,6 +432,29 @@
         )
         table = jnp.where(spread == at_own[:, 0:1], jax.nn.sigmoid(gap), 0.0)
         table = table + jnp.where(spread == at_own[:, 1:2], jax.nn.sigmoid(-gap), 0.0)
+
+        arrive(RP, P_TWIN[1])
+
+        def gains_of(device):
+            return gn[2:3, cut(device * block, block)]
+
+        FF[c] = (R[...].reshape(rows, block).astype(f32) * g2).astype(bf16)
+        FF[1 - c] = (RP[...].reshape(rows, block).astype(f32) * gains_of(partner)).astype(bf16)
+
+        def dense_part(j, ox, to):
+            piece = (dot32(FF[0], wd[j, 0]) + dot32(FF[1], wd[j, 1])).astype(bf16)
+            for kk in range(half):
+                ox[kk] = piece[kk * duo : (kk + 1) * duo]
+            to[q] = ox[q]
+
+        def dense_send(ox, to, s, r):
+            for kk in away:
+                put(ox.at[kk], to.at[q], (2 * kk + c, me_t), s, r)
+
+        for j in range(CHUNKS):
+            l_wd[j].wait()
+            arrive(wd.at[j, 0], P_SWAP[1] + j)
+        dense_part(0, AX, AR)
 
         l_st.wait()
         for h in range(heads):
@@ -459,9 +491,6 @@
                     P_MIX[1] + q,
                 )
 
-        for de, e in ep_peers:
-            put(OT.at[e], ET.at[:, mine], (e, me_t), P_ROWS[0], P_ROWS[1])
-
         def update(h):
             for s in range(seqs):
                 ns[s, h] = (
@@ -489,6 +518,9 @@
                     P_TP[0],
                     P_TP[1] + kk,
                 )
+        dense_send(AX, AR, *P_BASE)
+        for de, e in ep_peers:
+            put(OT.at[e], ET.at[:, mine], (e, me_t), P_ROWS[0], P_ROWS[1])
         lane_duo = lax.broadcasted_iota(i32, (duo, lanes), 1)
         mixer = jnp.concatenate(
             [
@@ -521,17 +553,22 @@
                     lane_duo == i, jnp.sum(figure, axis=1, keepdims=True), 0.0
                 )
             STAT[kk] = stat
+        put(MO, MP, (partner, me_t), P_TWIN[0], P_TWIN[1] + 1)
         SX[...] = STAT[...].reshape(rows, lanes).T[0:8, :]
         SR[me_e] = SX[...]
         for de, e in ep_peers:
             put(SX, SR.at[me_e], (e, me_t), P_STAT[0], P_STAT[1])
-        put(MO, MP, (partner, me_t), P_TWIN[0], P_TWIN[1] + 1)
-        picked = dot32(SEL[...], MO[...].reshape(rows, block)).astype(bf16)
-        for e in range(n_ep):
-            OX[e] = picked[e * cells : (e + 1) * cells]
+        pick(MO, OX)
         for de, e in ep_peers:
             put(OX.at[e], ER.at[:, mine], (e, me_t), P_EXP[0], P_EXP[1])
         ER[:, mine] = OX[me_e]
+
+        FF[c] = (MO[...].reshape(rows, block).astype(f32) * (g1 * g2)).astype(bf16)
+        arrive(MP, P_TWIN[1] + 1)
+        both = gn[1:2, cut(partner * block, block)] * gains_of(partner)
+        FF[1 - c] = (MP[...].reshape(rows, block).astype(f32) * both).astype(bf16)
+        dense_part(0, DX.at[0], DR.at[0])
+        dense_send(DX.at[0], DR.at[0], *P_DENSE)
 
         def send_own():
             for _, e in ep_peers:
@@ -548,8 +585,6 @@
         pl.when(holds)(send_own)
         update(2)
         update(3)
-        arrive(RP, P_TWIN[1])
-        arrive(MP, P_TWIN[1] + 1)
 
         arrive(SR.at[0:others], P_STAT[1])
         total = SR[0]
@@ -570,28 +605,38 @@
 
         FF[c] = normed(R, MO, me_e)
         FF[1 - c] = normed(RP, MP, partner)
-
-        for j in range(CHUNKS):
-            l_wd[j].wait()
-            arrive(wd.at[j, 0], P_SWAP[1] + j)
-            piece = (dot32(FF[0], wd[j, 0]) + dot32(FF[1], wd[j, 1])).astype(bf16)
-            for kk in range(half):
-                DX[j, kk] = piece[kk * duo : (kk + 1) * duo]
-            for kk in away:
-                put(
-                    DX.at[j, kk],
-                    DR.at[j, q],
-                    (2 * kk + c, me_t),
-                    P_DENSE[0],
-                    P_DENSE[1] + j,
-                )
-            DR[j, q] = DX[j, q]
+        for j in range(1, CHUNKS):
+            dense_part(j, DX.at[j], DR.at[j])
+            dense_send(DX.at[j], DR.at[j], P_DENSE[0], P_DENSE[1] + j)
+
+        arrive(OT.at[0:others], P_ROWS[1])
+        arrive(OX.at[0:others], P_EXP[1])
+        marks = jnp.dot(
+            SEL[me_e, me_t].astype(f32),
+            back,
+            precision=lax.Precision.HIGHEST,
+            preferred_element_type=f32,
+        )
+        share = pl.ds(pl.multiple_of(me_t * few, few), few)
+        after = ET[...].astype(f32) + ER[...].astype(f32) * marks[:, 0:1] * gn[1:2, :]
+        EI[share, :] = (after * marks[:, 1:2] * gn[2:3, :]).astype(bf16)
+        for dt, t in tp_peers:
+            put(EI.at[share], EI.at[share], (me_e, t), P_ALL[0], P_ALL[1])
+
+        chip_rows = pl.ds(pl.multiple_of(q * duo, duo), duo)
 
         def hidden(j):
             arrive(DR.at[j, 0:far], P_DENSE[1] + j)
             total = DR[j, 0].astype(f32)
             for kk in range(1, half):
                 total = total + DR[j, kk].astype(f32)
+            if j == 0:
+                arrive(AR.at[0:far], P_BASE[1])
+                base = AR[0].astype(f32)
+                for kk in range(1, half):
+                    base = base + AR[kk].astype(f32)
+                own = COL[chip_rows, :]
+                total = (base + own[:, 0:1] * total) * own[:, 1:2]
             here = DH.at[j, c, q]
             here[...] = (silu(total[:, :hc]) * total[:, hc:]).astype(bf16)
             for kk in away:
@@ -614,24 +659,17 @@
 
         for copy in l_exp:
             copy.wait()
-        arrive(OT.at[0:others], P_ROWS[1])
-        arrive(OX.at[0:others], P_EXP[1])
-        marks = jnp.dot(
-            SEL[pl.ds(pl.multiple_of(me_e * cells, cells), cells), :].astype(f32),
-            back,
-            precision=lax.Precision.HIGHEST,
-            preferred_element_type=f32,
-        )
-        for a in range(0, width, block):
-            at = slice(a, a + block)
-            after = ET[:, at].astype(f32) + ER[:, at].astype(f32) * marks[:, 0:1] * gn[1:2, at]
-            EI[:, at] = (after * marks[:, 1:2] * gn[2:3, at]).astype(bf16)
+        hidden(0)
+        hidden(1)
+        arrive(EI.at[0 : peers * few], P_ALL[1])
 
         @pl.loop(0, eff // tile)
         def _(i):
             both = dot32(EI[...], wgu[:, cut(i * 2 * tile, 2 * tile)])
             hid[:, cut(i * tile, tile)] = (silu(both[:, :tile]) * both[:, tile:]).astype(bf16)
 
+        for j in range(2, CHUNKS):
+            hidden(j)
         for dt, t in tp_peers + [(0, me_t)]:
             piece = dot32(hid[...], wed[:, cut(t * part, part)]).astype(bf16)
             if dt:
@@ -652,9 +690,6 @@
             for de, e in ep_peers:
                 put(RB.at[e], RG.at[me_e], (e, me_t), P_RET[0], P_RET[1])
 
-        for j in range(CHUNKS):
-            hidden(j)
-        give_back()
         for j in range(CHUNKS):
             hand_over(j)
         l_wdd.wait()
@@ -676,6 +711,8 @@
         pl.when(jnp.logical_not(holds))(
             lambda: put(dd.at[me_e], landing, (me_e, to), P_COLS[0], P_COLS[1])
         )
+
+        give_back()
 
         arrive(RG.at[0:others], P_RET[1])
         expert_sum = jnp.dot(
@@ -728,6 +765,8 @@
             (SR.at[0:others], P_STAT),
             (wd.at[:, 0], P_SWAP),
             (FF, P_TWIN),
+            (AX.at[0:far], P_BASE),
+            (EI.at[0 : peers * few], P_ALL),
             (OT.at[0:others], P_ROWS),
             (OX.at[0:others], P_EXP),
             (DX.at[:, 0:far], P_DENSE),
@@ -786,18 +825,20 @@
             f(n_ep, 8, lanes),
             f(rows, lanes),
             n(rows, lanes),
-            b(n_ep * cells, rows),
+            b(n_ep, n_tp, few, rows),
             b(n_ep, seqs, block),
             b(n_ep, seqs, block),
             b(ratio, seqs, block),
             b(2, rows, block),
+            b(half, duo, chunk),
+            b(half, duo, chunk),
             b(CHUNKS, half, duo, chunk),
             b(CHUNKS, half, duo, chunk),
             b(CHUNKS, 2, half, duo, hc),
-            b(n_ep, cells, block),
-            b(n_ep, cells, block),
-            b(cells, width),
-            b(cells, width),
+            b(n_ep, few, block),
+            b(n_ep, few, block),
+            b(few, width),
+            b(few, width),
             b(cells, width),
             b(cells, eff),
             b(n_tp, cells, part),

time: 63.6 us -> 58.4 us (0.918)
  Pallas kernels: 62.8 us -> 57.6 us
    pallas_call x1, Pallas kernels: 60.7 us -> 55.4 us  [fused_layer(): pl.pallas_call(kernel, out_shape=(jax.ShapeDtypeStruct((seqs, part), bf16...]
where the time goes in v4:
time: 58.4 us; the launch traced here: 58.2 us
  Pallas kernels  57.6 us (99%)
  between operations  0.65 us (1%)
    pallas_call x1, Pallas kernels, fused_layer(): pl.pallas_call(kernel, out_shape=(jax.ShapeDtypeStruct((seqs, part), bf16...  55.4 us
    pallas_call x1, Pallas kernels, write_out(): pl.pallas_call(kernel, out_shape=(pltpu.HBM(layer_out.shape, layer_out.dt...  2.15 us

profile of v4, /device:TPU:0, one launch (start us, length us, event | category | flops | bytes accessed | tf_op | source)
XLA Modules:
  0.0 58.2 jit_solution(5781468208313388601)
XLA Ops:
  0.6 55.4 %fused_layer.1 = (bf16[16,512]{1,0:T(8,128)(2,1)S(1)}, f32[16,4,128,128]{3,2,1,0:T(8,128)S(1)}) custom-call(bf16[16,2048]{1,0:T(8,128)(2,1)} %tok_h.1, f32[16,4,128,128]{3,2,1,0:T(8,128)} %st_h.1, f32[1,512]{1,0:T(1,128)} %bitcast.6, f32[1,512]{1,0:T(1,128)} %bitcast.7, f32[4,2048]{1,0:T(4,128)} %gn_h.1, bf16[256,512]{1,0:T(8,128)(2,1)} %wq_h.1, ...), custom_call_target="tpu_custom_call" | custom-call | tf_op jit(solution)/shard_map/fused_layer/pallas_call | solution.py:786
  56.1 2.1 %write_out.1 = (bf16[16,512]{1,0:T(8,128)(2,1)}, f32[16,4,128,128]{3,2,1,0:T(8,128)}) custom-call(bf16[16,512]{1,0:T(8,128)(2,1)S(1)} %get-tuple-element.4.small, f32[16,4,128,128]{3,2,1,0:T(8,128)S(1)} %get-tuple-element.5.big), custom_call_target="tpu_custom_call" | custom-call | tf_op jit(solution)/shard_map/write_out/pallas_call | solution.py:899

commit v5 on v4

--- a/solution.py
+++ b/solution.py
@@ -174,6 +174,7 @@
 
 
 CHUNKS = 3
+EARLY = 1
 
 
 def fused_layer(
@@ -236,8 +237,13 @@
         partner = 2 * q + 1 - c
         chips = chips_by_distance(q, half)
         away = chips[:0:-1]
-        ep_peers = [(de, lax.rem(me_e + de, n_ep)) for de in range(1, n_ep)]
-        tp_peers = [(dt, lax.rem(me_t + dt, n_tp)) for dt in range(1, n_tp)]
+        far_first = [2 * kk + d for kk in away for d in (c, 1 - c)] + [partner]
+        ep_peers = list(enumerate(far_first, 1))
+        if n_tp == 4:
+            turn_tp = [n_tp - 1 - me_t, lax.rem(me_t + 2, n_tp), me_t + 1 - 2 * lax.rem(me_t, 2)]
+        else:
+            turn_tp = [lax.rem(me_t + dt, n_tp) for dt in range(1, n_tp)]
+        tp_peers = list(enumerate(turn_tp, 1))
 
         barrier = pltpu.get_barrier_semaphore()
         for _, e in ep_peers:
@@ -454,7 +460,8 @@
         for j in range(CHUNKS):
             l_wd[j].wait()
             arrive(wd.at[j, 0], P_SWAP[1] + j)
-        dense_part(0, AX, AR)
+        for j in range(EARLY):
+            dense_part(j, AX.at[j], AR.at[j])
 
         l_st.wait()
         for h in range(heads):
@@ -500,6 +507,8 @@
 
         update(0)
         update(1)
+        for de, e in ep_peers:
+            put(OT.at[e], ET.at[:, mine], (e, me_t), P_ROWS[0], P_ROWS[1])
 
         l_wm.wait()
         for g, kk in enumerate(chips):
@@ -518,9 +527,8 @@
                     P_TP[0],
                     P_TP[1] + kk,
                 )
-        dense_send(AX, AR, *P_BASE)
-        for de, e in ep_peers:
-            put(OT.at[e], ET.at[:, mine], (e, me_t), P_ROWS[0], P_ROWS[1])
+        for j in range(EARLY):
+            dense_send(AX.at[j], AR.at[j], *P_BASE)
         lane_duo = lax.broadcasted_iota(i32, (duo, lanes), 1)
         mixer = jnp.concatenate(
             [
@@ -567,8 +575,9 @@
         arrive(MP, P_TWIN[1] + 1)
         both = gn[1:2, cut(partner * block, block)] * gains_of(partner)
         FF[1 - c] = (MP[...].reshape(rows, block).astype(f32) * both).astype(bf16)
-        dense_part(0, DX.at[0], DR.at[0])
-        dense_send(DX.at[0], DR.at[0], *P_DENSE)
+        for j in range(EARLY):
+            dense_part(j, DX.at[j], DR.at[j])
+            dense_send(DX.at[j], DR.at[j], P_DENSE[0], P_DENSE[1] + j)
 
         def send_own():
             for _, e in ep_peers:
@@ -605,7 +614,7 @@
 
         FF[c] = normed(R, MO, me_e)
         FF[1 - c] = normed(RP, MP, partner)
-        for j in range(1, CHUNKS):
+        for j in range(EARLY, CHUNKS):
             dense_part(j, DX.at[j], DR.at[j])
             dense_send(DX.at[j], DR.at[j], P_DENSE[0], P_DENSE[1] + j)
 
@@ -631,10 +640,11 @@
             for kk in range(1, half):
                 total = total + DR[j, kk].astype(f32)
             if j == 0:
-                arrive(AR.at[0:far], P_BASE[1])
-                base = AR[0].astype(f32)
+                arrive(AR.at[:, 0:far], P_BASE[1])
+            if j < EARLY:
+                base = AR[j, 0].astype(f32)
                 for kk in range(1, half):
-                    base = base + AR[kk].astype(f32)
+                    base = base + AR[j, kk].astype(f32)
                 own = COL[chip_rows, :]
                 total = (base + own[:, 0:1] * total) * own[:, 1:2]
             here = DH.at[j, c, q]
@@ -660,7 +670,6 @@
         for copy in l_exp:
             copy.wait()
         hidden(0)
-        hidden(1)
         arrive(EI.at[0 : peers * few], P_ALL[1])
 
         @pl.loop(0, eff // tile)
@@ -668,8 +677,7 @@
             both = dot32(EI[...], wgu[:, cut(i * 2 * tile, 2 * tile)])
             hid[:, cut(i * tile, tile)] = (silu(both[:, :tile]) * both[:, tile:]).astype(bf16)
 
-        for j in range(2, CHUNKS):
-            hidden(j)
+        hidden(1)
         for dt, t in tp_peers + [(0, me_t)]:
             piece = dot32(hid[...], wed[:, cut(t * part, part)]).astype(bf16)
             if dt:
@@ -677,6 +685,7 @@
                 put(RX.at[dt], RR.at[me_t], (me_e, t), P_RTP[0], P_RTP[1])
             else:
                 RR[me_t] = piece
+        hidden(2)
 
         def give_back():
             arrive(RR.at[0:peers], P_RTP[1])
@@ -692,6 +701,7 @@
 
         for j in range(CHUNKS):
             hand_over(j)
+        give_back()
         l_wdd.wait()
         total = gathered(0)
         for j in range(1, CHUNKS):
@@ -711,8 +721,6 @@
         pl.when(jnp.logical_not(holds))(
             lambda: put(dd.at[me_e], landing, (me_e, to), P_COLS[0], P_COLS[1])
         )
-
-        give_back()
 
         arrive(RG.at[0:others], P_RET[1])
         expert_sum = jnp.dot(
@@ -765,7 +773,7 @@
             (SR.at[0:others], P_STAT),
             (wd.at[:, 0], P_SWAP),
             (FF, P_TWIN),
-            (AX.at[0:far], P_BASE),
+            (AX.at[:, 0:far], P_BASE),
             (EI.at[0 : peers * few], P_ALL),
             (OT.at[0:others], P_ROWS),
             (OX.at[0:others], P_EXP),
@@ -830,8 +838,8 @@
             b(n_ep, seqs, block),
             b(ratio, seqs, block),
             b(2, rows, block),
-            b(half, duo, chunk),
-            b(half, duo, chunk),
+            b(EARLY, half, duo, chunk),
+            b(EARLY, half, duo, chunk),
             b(CHUNKS, half, duo, chunk),
             b(CHUNKS, half, duo, chunk),
             b(CHUNKS, 2, half, duo, hc),

time: 58.4 us -> 57.4 us (0.983)
  Pallas kernels: 57.6 us -> 56.6 us
    pallas_call x1, Pallas kernels: 55.4 us -> 54.4 us  [fused_layer(): pl.pallas_call(kernel, out_shape=(jax.ShapeDtypeStruct((seqs, part), bf16...]
where the time goes in v5:
time: 57.4 us; the launch traced here: 57.2 us
  Pallas kernels  56.6 us (99%)
  between operations  0.65 us (1%)
    pallas_call x1, Pallas kernels, fused_layer(): pl.pallas_call(kernel, out_shape=(jax.ShapeDtypeStruct((seqs, part), bf16...  54.4 us
    pallas_call x1, Pallas kernels, write_out(): pl.pallas_call(kernel, out_shape=(pltpu.HBM(layer_out.shape, layer_out.dt...  2.15 us

profile of v5, /device:TPU:0, one launch (start us, length us, event | category | flops | bytes accessed | tf_op | source)
XLA Modules:
  0.0 57.2 jit_solution(16567867422537159255)
XLA Ops:
  0.6 54.4 %fused_layer.1 = (bf16[16,512]{1,0:T(8,128)(2,1)S(1)}, f32[16,4,128,128]{3,2,1,0:T(8,128)S(1)}) custom-call(bf16[16,2048]{1,0:T(8,128)(2,1)} %tok_h.1, f32[16,4,128,128]{3,2,1,0:T(8,128)} %st_h.1, f32[1,512]{1,0:T(1,128)} %bitcast.6, f32[1,512]{1,0:T(1,128)} %bitcast.7, f32[4,2048]{1,0:T(4,128)} %gn_h.1, bf16[256,512]{1,0:T(8,128)(2,1)} %wq_h.1, ...), custom_call_target="tpu_custom_call" | custom-call | tf_op jit(solution)/shard_map/fused_layer/pallas_call | solution.py:794
  55.1 2.1 %write_out.1 = (bf16[16,512]{1,0:T(8,128)(2,1)}, f32[16,4,128,128]{3,2,1,0:T(8,128)}) custom-call(bf16[16,512]{1,0:T(8,128)(2,1)S(1)} %get-tuple-element.4.small, f32[16,4,128,128]{3,2,1,0:T(8,128)S(1)} %get-tuple-element.5.big), custom_call_target="tpu_custom_call" | custom-call | tf_op jit(solution)/shard_map/write_out/pallas_call | solution.py:907

commit v6 on v5

--- a/solution.py
+++ b/solution.py
@@ -216,6 +216,7 @@
         return send_at.take(1), recv_at.take(count)
 
     P_TOK, P_ROUTE, P_PAIR, P_HEAD = pair(1), pair(1), pair(heads), pair(heads)
+    V_DENSE = recv_at.take(CHUNKS)
     P_MIX, P_TP, P_STAT, P_OWN = pair(half), pair(half), pair(1), pair(ratio)
     P_SWAP, P_TWIN, P_BASE, P_DENSE = pair(CHUNKS), pair(2), pair(1), pair(CHUNKS)
     P_ROWS, P_EXP, P_ALL = pair(1), pair(1), pair(1)
@@ -228,7 +229,7 @@
         eg_h, eu_h, ed_h, dg_h, du_h, dd_h, mr_h,
         out, ns,
         tok, st, lb, hg, gn, win, wm, rt0, sc, wgu, wed, wd, wdd, mrow, wide_row,
-        R, RP, RT, X, Y, Z, PR, rd, KC, VL, MA, TX, TR, STAT, SX, SR, COL, OWN, SEL, MO, MP, MR,
+        R, RP, RT, X, Y, Z, VD, PR, rd, KC, VL, MA, TX, TR, STAT, SX, SR, COL, OWN, SEL, MO, MP, MR,
         FF, AX, AR, DX, DR, DH, OT, OX, ET, ER, EI, hid, RX, RR, RB, RG, dd, ddr, sq, sqr,
         send, recv, lsem,
     ):
@@ -237,6 +238,43 @@
         partner = 2 * q + 1 - c
         chips = chips_by_distance(q, half)
         away = chips[:0:-1]
+        line = half == 4
+        at_end = lax.rem(q, 3) == 0
+        beside = 1 + q // 3
+        near = away[1:] if line else away
+
+        def landed(ref, r):
+            if line:
+                pl.when(at_end)(lambda: arrive(ref.at[0 : far - 1], r))
+                pl.when(jnp.logical_not(at_end))(lambda: arrive(ref.at[0:far], r))
+            else:
+                arrive(ref.at[0:far], r)
+
+        def through(ox, via, s, r):
+            if line:
+                pl.when(at_end)(
+                    lambda: put(ox.at[away[0]], via, (2 * beside + c, me_t), s, r)
+                )
+
+        def relay(j):
+            def run():
+                arrive(VD.at[j], V_DENSE + j)
+                total = DX[j, away[0]].astype(f32) + VD[j].astype(f32)
+                DX[j, away[0]] = total.astype(bf16)
+                put(
+                    DX.at[j, away[0]],
+                    DR.at[j, q],
+                    (2 * away[0] + c, me_t),
+                    P_DENSE[0],
+                    P_DENSE[1] + j,
+                )
+
+            def clear():
+                DR[j, away[0]] = jnp.zeros((duo, chunk), bf16)
+
+            if line:
+                pl.when(jnp.logical_not(at_end))(run)
+                pl.when(at_end)(clear)
         far_first = [2 * kk + d for kk in away for d in (c, 1 - c)] + [partner]
         ep_peers = list(enumerate(far_first, 1))
         if n_tp == 4:
@@ -453,8 +491,8 @@
                 ox[kk] = piece[kk * duo : (kk + 1) * duo]
             to[q] = ox[q]
 
-        def dense_send(ox, to, s, r):
-            for kk in away:
+        def dense_send(ox, to, s, r, direct=away):
+            for kk in direct:
                 put(ox.at[kk], to.at[q], (2 * kk + c, me_t), s, r)
 
         for j in range(CHUNKS):
@@ -577,7 +615,8 @@
         FF[1 - c] = (MP[...].reshape(rows, block).astype(f32) * both).astype(bf16)
         for j in range(EARLY):
             dense_part(j, DX.at[j], DR.at[j])
-            dense_send(DX.at[j], DR.at[j], P_DENSE[0], P_DENSE[1] + j)
+            through(DX.at[j], VD.at[j], P_DENSE[0], V_DENSE + j)
+            dense_send(DX.at[j], DR.at[j], P_DENSE[0], P_DENSE[1] + j, near)
 
         def send_own():
             for _, e in ep_peers:
@@ -594,6 +633,8 @@
         pl.when(holds)(send_own)
         update(2)
         update(3)
+        for j in range(EARLY):
+            relay(j)
 
         arrive(SR.at[0:others], P_STAT[1])
         total = SR[0]
@@ -616,7 +657,9 @@
         FF[1 - c] = normed(RP, MP, partner)
         for j in range(EARLY, CHUNKS):
             dense_part(j, DX.at[j], DR.at[j])
-            dense_send(DX.at[j], DR.at[j], P_DENSE[0], P_DENSE[1] + j)
+            through(DX.at[j], VD.at[j], P_DENSE[0], V_DENSE + j)
+        for j in range(EARLY, CHUNKS):
+            dense_send(DX.at[j], DR.at[j], P_DENSE[0], P_DENSE[1] + j, near)
 
         arrive(OT.at[0:others], P_ROWS[1])
         arrive(OX.at[0:others], P_EXP[1])
@@ -632,10 +675,12 @@
         for dt, t in tp_peers:
             put(EI.at[share], EI.at[share], (me_e, t), P_ALL[0], P_ALL[1])
 
+        for j in range(EARLY, CHUNKS):
+            relay(j)
         chip_rows = pl.ds(pl.multiple_of(q * duo, duo), duo)
 
         def hidden(j):
-            arrive(DR.at[j, 0:far], P_DENSE[1] + j)
+            landed(DR.at[j], P_DENSE[1] + j)
             total = DR[j, 0].astype(f32)
             for kk in range(1, half):
                 total = total + DR[j, kk].astype(f32)
@@ -678,7 +723,7 @@
             hid[:, cut(i * tile, tile)] = (silu(both[:, :tile]) * both[:, tile:]).astype(bf16)
 
         hidden(1)
-        for dt, t in tp_peers + [(0, me_t)]:
+        for dt, t in (tp_peers + [(0, me_t)])[:2]:
             piece = dot32(hid[...], wed[:, cut(t * part, part)]).astype(bf16)
             if dt:
                 RX[dt] = piece
@@ -686,6 +731,13 @@
             else:
                 RR[me_t] = piece
         hidden(2)
+        for dt, t in (tp_peers + [(0, me_t)])[2:]:
+            piece = dot32(hid[...], wed[:, cut(t * part, part)]).astype(bf16)
+            if dt:
+                RX[dt] = piece
+                put(RX.at[dt], RR.at[me_t], (me_e, t), P_RTP[0], P_RTP[1])
+            else:
+                RR[me_t] = piece
 
         def give_back():
             arrive(RR.at[0:peers], P_RTP[1])
@@ -821,6 +873,7 @@
             b(heads, 2, half, seqs, 4 * hs),
             b(heads, half, seqs, 4 * hs),
             b(heads, half, seqs, 4 * hs),
+            b(CHUNKS, duo, chunk),
             b(heads, half, seqs, 4 * hs),
             f(seqs, hs),
             f(heads, hs, hs),

time: 57.4 us -> 56.1 us (0.977)
  Pallas kernels: 56.6 us -> 55.3 us
    pallas_call x1, Pallas kernels: 54.4 us -> 53.1 us  [fused_layer(): pl.pallas_call(kernel, out_shape=(jax.ShapeDtypeStruct((seqs, part), bf16...]
where the time goes in v6:
time: 56.1 us; the launch traced here: 55.9 us
  Pallas kernels  55.3 us (99%)
  between operations  0.65 us (1%)
    pallas_call x1, Pallas kernels, fused_layer(): pl.pallas_call(kernel, out_shape=(jax.ShapeDtypeStruct((seqs, part), bf16...  53.1 us
    pallas_call x1, Pallas kernels, write_out(): pl.pallas_call(kernel, out_shape=(pltpu.HBM(layer_out.shape, layer_out.dt...  2.15 us

profile of v6, /device:TPU:0, one launch (start us, length us, event | category | flops | bytes accessed | tf_op | source)
XLA Modules:
  0.0 55.9 jit_solution(15459147080907294641)
XLA Ops:
  0.6 53.1 %fused_layer.1 = (bf16[16,512]{1,0:T(8,128)(2,1)S(1)}, f32[16,4,128,128]{3,2,1,0:T(8,128)S(1)}) custom-call(bf16[16,2048]{1,0:T(8,128)(2,1)} %tok_h.1, f32[16,4,128,128]{3,2,1,0:T(8,128)} %st_h.1, f32[1,512]{1,0:T(1,128)} %bitcast.6, f32[1,512]{1,0:T(1,128)} %bitcast.7, f32[4,2048]{1,0:T(4,128)} %gn_h.1, bf16[256,512]{1,0:T(8,128)(2,1)} %wq_h.1, ...), custom_call_target="tpu_custom_call" | custom-call | tf_op jit(solution)/shard_map/fused_layer/pallas_call | solution.py:846
  53.8 2.1 %write_out.1 = (bf16[16,512]{1,0:T(8,128)(2,1)}, f32[16,4,128,128]{3,2,1,0:T(8,128)}) custom-call(bf16[16,512]{1,0:T(8,128)(2,1)S(1)} %get-tuple-element.4.small, f32[16,4,128,128]{3,2,1,0:T(8,128)S(1)} %get-tuple-element.5.big), custom_call_target="tpu_custom_call" | custom-call | tf_op jit(solution)/shard_map/write_out/pallas_call | solution.py:960

commit v7 on v6

--- a/solution.py
+++ b/solution.py
@@ -218,11 +218,11 @@
     P_TOK, P_ROUTE, P_PAIR, P_HEAD = pair(1), pair(1), pair(heads), pair(heads)
     V_DENSE = recv_at.take(CHUNKS)
     P_MIX, P_TP, P_STAT, P_OWN = pair(half), pair(half), pair(1), pair(ratio)
-    P_SWAP, P_TWIN, P_BASE, P_DENSE = pair(CHUNKS), pair(2), pair(1), pair(CHUNKS)
-    P_ROWS, P_EXP, P_ALL = pair(1), pair(1), pair(1)
+    P_SWAP, P_TWIN, P_BASE, P_DENSE = pair(1), pair(2), pair(1), pair(CHUNKS)
+    P_ROWS, P_EXP, P_ALL = pair(1), pair(1), pair(2)
     P_RTP, P_RET = pair(1), pair(1)
     P_GATH, P_HAND, P_COLS, P_SQ = pair(CHUNKS), pair(CHUNKS), pair(1), pair(1)
-    n_load = 13 + CHUNKS
+    n_load = 14
 
     def kernel(
         tok_h, st_h, lb_h, hg_h, gn_h, wq_h, wf_h, wv_h, wo_h, wm_h, rt_h, sc_h,
@@ -230,7 +230,7 @@
         out, ns,
         tok, st, lb, hg, gn, win, wm, rt0, sc, wgu, wed, wd, wdd, mrow, wide_row,
         R, RP, RT, X, Y, Z, VD, PR, rd, KC, VL, MA, TX, TR, STAT, SX, SR, COL, OWN, SEL, MO, MP, MR,
-        FF, AX, AR, DX, DR, DH, OT, OX, ET, ER, EI, hid, RX, RR, RB, RG, dd, ddr, sq, sqr,
+        FF, AX, AR, DX, DR, DH, OT, OX, ET, ER, EI, acc, hid, RX, RR, RB, RG, dd, ddr, sq, sqr,
         send, recv, lsem,
     ):
         me_e, me_t = lax.axis_index("ep"), lax.axis_index("tp")
@@ -288,6 +288,9 @@
             pl.semaphore_signal(barrier, inc=1, device_id=(e, me_t), device_id_type=MESH)
         for _, t in tp_peers:
             pl.semaphore_signal(barrier, inc=1, device_id=(me_e, t), device_id_type=MESH)
+
+        def cut(first, size):
+            return pl.ds(pl.multiple_of(first, 128), size)
 
         count = [0]
 
@@ -314,19 +317,17 @@
         ]
         l_st = load(st, (st_h, st))
         l_wm = load(wm, (wm_h, wm))
-        l_wd = [
-            load(
-                wd.at[j, 0],
-                *(
-                    (
-                        w.at[:, pl.ds(pl.multiple_of(j * chunk + c * hc, 128), hc)],
-                        wd.at[j, c, :, i * hc : (i + 1) * hc],
-                    )
-                    for i, w in enumerate((dg_h, du_h))
-                ),
-            )
-            for j in range(CHUNKS)
-        ]
+        l_wd = load(
+            wd.at[:, 0],
+            *(
+                (
+                    w.at[:, cut(j * chunk + c * hc, hc)],
+                    wd.at[j, c, :, i * hc : (i + 1) * hc],
+                )
+                for j in range(CHUNKS)
+                for i, w in enumerate((dg_h, du_h))
+            ),
+        )
         l_exp = [
             load(
                 wgu,
@@ -361,9 +362,6 @@
 
         others, peers, far = n_ep - 1, n_tp - 1, half - 1
 
-        def cut(first, size):
-            return pl.ds(pl.multiple_of(first, 128), size)
-
         mine = cut(me_e * block, block)
         own_rows = pl.ds(pl.multiple_of(me_e * seqs, seqs), seqs)
 
@@ -382,7 +380,7 @@
                     wd.at[j, c, :, i * hc : (i + 1) * hc],
                     (partner, me_t),
                     P_SWAP[0],
-                    P_SWAP[1] + j,
+                    P_SWAP[1],
                 )
         R[me_e] = tok[:, mine]
         RT[me_e] = rt0[...]
@@ -495,9 +493,8 @@
             for kk in direct:
                 put(ox.at[kk], to.at[q], (2 * kk + c, me_t), s, r)
 
-        for j in range(CHUNKS):
-            l_wd[j].wait()
-            arrive(wd.at[j, 0], P_SWAP[1] + j)
+        l_wd.wait()
+        arrive(wd.at[:, 0], P_SWAP[1])
         for j in range(EARLY):
             dense_part(j, AX.at[j], AR.at[j])
 
@@ -670,10 +667,13 @@
             preferred_element_type=f32,
         )
         share = pl.ds(pl.multiple_of(me_t * few, few), few)
-        after = ET[...].astype(f32) + ER[...].astype(f32) * marks[:, 0:1] * gn[1:2, :]
-        EI[share, :] = (after * marks[:, 1:2] * gn[2:3, :]).astype(bf16)
-        for dt, t in tp_peers:
-            put(EI.at[share], EI.at[share], (me_e, t), P_ALL[0], P_ALL[1])
+        sides = (slice(0, width // 2), slice(width // 2, width))
+        for i, side in enumerate(sides):
+            after = ET[:, side].astype(f32) + ER[:, side].astype(f32) * marks[:, 0:1] * gn[1:2, side]
+            EI[share, side] = (after * marks[:, 1:2] * gn[2:3, side]).astype(bf16)
+            for dt, t in tp_peers:
+                here = EI.at[share, side]
+                put(here, here, (me_e, t), P_ALL[0], P_ALL[1] + i)
 
         for j in range(EARLY, CHUNKS):
             relay(j)
@@ -715,11 +715,19 @@
         for copy in l_exp:
             copy.wait()
         hidden(0)
-        arrive(EI.at[0 : peers * few], P_ALL[1])
+        arrive(EI.at[0 : peers * few, sides[0]], P_ALL[1])
 
         @pl.loop(0, eff // tile)
         def _(i):
-            both = dot32(EI[...], wgu[:, cut(i * 2 * tile, 2 * tile)])
+            at = cut(i * 2 * tile, 2 * tile)
+            acc[:, at] = dot32(EI[:, sides[0]], wgu[sides[0], at])
+
+        arrive(EI.at[0 : peers * few, sides[1]], P_ALL[1] + 1)
+
+        @pl.loop(0, eff // tile)
+        def _(i):
+            at = cut(i * 2 * tile, 2 * tile)
+            both = acc[:, at] + dot32(EI[:, sides[1]], wgu[sides[1], at])
             hid[:, cut(i * tile, tile)] = (silu(both[:, :tile]) * both[:, tile:]).astype(bf16)
 
         hidden(1)
@@ -901,6 +909,7 @@
             b(few, width),
             b(few, width),
             b(cells, width),
+            f(cells, 2 * eff),
             b(cells, eff),
             b(n_tp, cells, part),
             b(n_tp, cells, part),

time: 56.1 us -> 56.1 us (level)
  no operation moved by 1% of the time
where the time goes in v7:
time: 56.1 us; the launch traced here: 55.9 us
  Pallas kernels  55.3 us (99%)
  between operations  0.65 us (1%)
    pallas_call x1, Pallas kernels, fused_layer(): pl.pallas_call(kernel, out_shape=(jax.ShapeDtypeStruct((seqs, part), bf16...  53.1 us
    pallas_call x1, Pallas kernels, write_out(): pl.pallas_call(kernel, out_shape=(pltpu.HBM(layer_out.shape, layer_out.dt...  2.15 us

profile of v7, /device:TPU:0, one launch (start us, length us, event | category | flops | bytes accessed | tf_op | source)
XLA Modules:
  0.0 55.9 jit_solution(12344496558891233076)
XLA Ops:
  0.6 53.1 %fused_layer.1 = (bf16[16,512]{1,0:T(8,128)(2,1)S(1)}, f32[16,4,128,128]{3,2,1,0:T(8,128)S(1)}) custom-call(bf16[16,2048]{1,0:T(8,128)(2,1)} %tok_h.1, f32[16,4,128,128]{3,2,1,0:T(8,128)} %st_h.1, f32[1,512]{1,0:T(1,128)} %bitcast.6, f32[1,512]{1,0:T(1,128)} %bitcast.7, f32[4,2048]{1,0:T(4,128)} %gn_h.1, bf16[256,512]{1,0:T(8,128)(2,1)} %wq_h.1, ...), custom_call_target="tpu_custom_call" | custom-call | tf_op jit(solution)/shard_map/fused_layer/pallas_call | solution.py:854
  53.8 2.1 %write_out.1 = (bf16[16,512]{1,0:T(8,128)(2,1)}, f32[16,4,128,128]{3,2,1,0:T(8,128)}) custom-call(bf16[16,512]{1,0:T(8,128)(2,1)S(1)} %get-tuple-element.4.small, f32[16,4,128,128]{3,2,1,0:T(8,128)S(1)} %get-tuple-element.5.big), custom_call_target="tpu_custom_call" | custom-call | tf_op jit(solution)/shard_map/write_out/pallas_call | solution.py:969
